TPU v7x, 256 devices: a whole 4x4x8 slice. The times are simulated.
256 devices in a mesh: sp: 32 (over z, y), tp: 8 (over x, core).
Axes of the slice: x: 4, y: 4, z: 8, core: 2. Of those that a mesh axis runs over, the one named last changes fastest.
Arguments:
- hidden: bfloat16 [24576, 2048], P(('sp', 'tp')), may hold values from -6 to 6
- norm_gain: float32 [2, 2048], replicated, may hold values from 0.1 to 1.9
- w_value: bfloat16 [2, 2048, 2048], P(None, 'sp', 'tp'), may hold values from -0.125 to 0.125
- w_gate: bfloat16 [2, 2048, 2048], P(None, 'sp', 'tp'), may hold values from -0.125 to 0.125
- conv_weight: float32 [2, 31, 2048], P(None, None, 'tp'), may hold values from -3 to 3
- conv_bias: float32 [2, 2048], P(None, 'tp'), may hold values from -3 to 3
- chan_gain: float32 [2, 2048], P(None, 'tp'), may hold values from 0.1 to 1.9
- chan_shift: float32 [2, 2048], P(None, 'tp'), may hold values from -3 to 3
- w_out: bfloat16 [2, 2048, 2048], P(None, 'tp', 'sp'), may hold values from -0.125 to 0.125
Outputs:
- result: bfloat16 [24576, 2048], P(('sp', 'tp'))
All inputs are finite; a program needn't handle non-finite values.
Results may differ from a plain program's by a relative error of at most 0.015.
Values may be sent and summed in bfloat16 or wider, within the bound.
No kernel may reach another device: no remote copies, remote signals or barrier semaphores. Data moves between devices by JAX's collectives and lax.ppermute only.
A program may use at most 64 MiB of HBM per device.

v0:
```python
import functools

import jax
import jax.numpy as jnp
from jax import lax
from jax.experimental import pallas as pl
from jax.experimental.pallas import tpu as pltpu
from jax.sharding import Mesh
from jax.sharding import PartitionSpec as P


SP = ("z", "y")
SP_TP = ("z", "y", "x", "c")
EPS = 1e-06
BF = jnp.bfloat16
F32 = jnp.float32
ROWS = 96
CH = 256
TAPS = 31
KEEP = 32
REST = ROWS - KEEP
WIDTH = 2048
CHANNELS = 2048
BUNDLE = 3 * CH
PIECE = 64


def take(a, axis, by):
    n = lax.axis_size(axis)
    return lax.ppermute(a, axis, [((i + by) % n, i) for i in range(n)])


def swap(a):
    return lax.ppermute(a, "c", [(0, 1), (1, 0)])


def call(kernel, outs, inputs, scratch=(), scalars=True):
    n = len(inputs) - (1 if scalars else 0)
    vmem = pl.BlockSpec(memory_space=pltpu.VMEM)
    specs = ([pl.BlockSpec(memory_space=pltpu.SMEM)] if scalars else []) + [vmem] * n
    return pl.pallas_call(
        kernel,
        out_shape=[jax.ShapeDtypeStruct(s, d) for s, d in outs],
        in_specs=specs,
        out_specs=[vmem] * len(outs),
        scratch_shapes=list(scratch),
        compiler_params=pltpu.CompilerParams(vmem_limit_bytes=12 * 1024 * 1024),
    )(*inputs)


def fold_kernel(at, gain, wv, wg, wo, b0, b1, col):
    sp = at[0] * 4 + at[1]
    for layer, out in ((0, b0), (1, b1)):
        lane = pl.multiple_of((sp // 2) * 128, 128)
        g = gain[layer : layer + 1, pl.ds(lane, 128)]
        col[...] = jnp.broadcast_to(g, (128, 128)).T
        g = col[pl.ds(pl.multiple_of((sp % 2) * PIECE, PIECE), PIECE), 0:1]
        out[:, :CH] = (wv[layer].astype(F32) * g).astype(BF)
        out[:, CH : 2 * CH] = (wg[layer].astype(F32) * g).astype(BF)
        out[:, 2 * CH :] = wo[layer]


def roll_kernel(at, hidden, state):
    for k in range(8):
        src = pl.multiple_of(((at[0] + k) % 8) * CH, CH)
        state[:, k * CH : (k + 1) * CH] = hidden[:, pl.ds(src, CH)]


def par_kernel(cw, cb, cg, cs, par):
    for layer in range(2):
        par[layer, :TAPS] = cw[:, layer]
        for n, a in enumerate((cb, cg, cs)):
            par[layer, TAPS + n : TAPS + n + 1] = a[layer : layer + 1]


def near_kernel(at, a0, a1, a2, a3, out):
    y = at[1]
    for k, a in enumerate((a0, a1, a2, a3)):
        out[pl.ds(pl.multiple_of(((y + k) % 4) * PIECE, PIECE), PIECE)] = a[...]


def line_kernel(own, za, zb, z2, z4, z6, out):
    pieces = (own, za, z2.at[:PIECE], z2.at[PIECE:], z4, z6.at[PIECE:], z6.at[:PIECE], zb)
    for k, a in enumerate(pieces):
        out[k * PIECE : (k + 1) * PIECE] = a[...]


def cat_kernel(*refs):
    out = refs[-1]
    for k, a in enumerate(refs[:8]):
        out[k * CH : (k + 1) * CH] = a[...]


def spread(at, refs, table, dst, lanes, out_lanes):
    for i, r, place, n in table:
        base, step = place, PIECE
        if isinstance(place, tuple):
            base, step = place[1] * CH + ((at[1] + place[0]) % 4) * PIECE, CH

        def piece(j, _, i=i, r=r, base=base, step=step):
            src = pl.multiple_of(r + j * PIECE, PIECE)
            to = pl.multiple_of(base + j * step, PIECE)
            dst[pl.ds(to, PIECE), out_lanes] = refs[i][pl.ds(src, PIECE), lanes]
            return 0

        lax.fori_loop(0, n // PIECE, piece, 0)


def glu_first_kernel(*refs, n, table):
    at, own, m, f, p = refs[:5]
    w = refs[5 : 5 + n]
    glu, tok, scale, full = refs[5 + n :]
    for r, a in enumerate((own, m, f, p)):
        tok[r * ROWS : (r + 1) * ROWS] = a[...]
        t = jnp.zeros((ROWS, 128), F32)
        for k in range(WIDTH // 128):
            v = a[:, k * 128 : (k + 1) * 128].astype(F32)
            t = t + v * v
        s = lax.rsqrt(jnp.sum(t, axis=1, keepdims=True) * (1.0 / WIDTH) + EPS)
        scale[r * ROWS : (r + 1) * ROWS] = jnp.broadcast_to(s, (ROWS, 128))
    spread(at, w, table, full, slice(0, 2 * CH), slice(0, 2 * CH))
    both = jnp.dot(tok[...], full[...], preferred_element_type=F32)
    s = scale[:, 0:1]
    lin, gate = both[:, :CH] * s, both[:, CH:] * s
    glu[...] = (lin / (1.0 + jnp.exp(-gate))).astype(BF)


def glu_second_kernel(*refs, n, table):
    at, tok, scale, other = refs[:4]
    w = refs[4 : 4 + n]
    glu, tails, last, full = refs[4 + n :]
    spread(at, w, table, full, slice(0, 2 * CH), slice(0, 2 * CH))
    both = jnp.dot(tok[...], full[...], preferred_element_type=F32)
    s = scale[:, 0:1]
    lin, gate = both[:, :CH] * s, both[:, CH:] * s
    glu[...] = (lin / (1.0 + jnp.exp(-gate))).astype(BF)
    for r in range(4):
        here = slice((r + 1) * ROWS - KEEP, (r + 1) * ROWS)
        tails[r * KEEP : (r + 1) * KEEP, :CH] = other[here]
        tails[r * KEEP : (r + 1) * KEEP, CH:] = glu[here]
    last[...] = tails[pl.ds(pl.multiple_of(((at[2] + 1) % 4) * KEEP, KEEP), KEEP)]


def glu_calls(at, tokens, own, other):
    (a, ta), (b, tb) = own, other
    size = (4 * ROWS, CH)
    full = pltpu.VMEM((WIDTH, 2 * CH), BF)
    glu_a, tok, scale = call(
        functools.partial(glu_first_kernel, n=len(a), table=ta),
        [(size, BF), ((4 * ROWS, WIDTH), BF), ((4 * ROWS, 128), F32)],
        [at, *tokens, *a],
        [full],
    )
    glu_b, tails, last = call(
        functools.partial(glu_second_kernel, n=len(b), table=tb),
        [(size, BF), ((4 * KEEP, 2 * CH), BF), ((KEEP, 2 * CH), BF)],
        [at, tok, scale, glu_a, *b],
        [full],
    )
    return glu_a, glu_b, tails, last


def conv_strip(win, par, lanes, rows):
    acc = jnp.zeros((rows, 128), F32) + par[TAPS : TAPS + 1, lanes]
    for s in range(8):
        shifted = win[s : s + rows + (24 if s else 32)]
        for base in range(0, 40, 8):
            tap = base + s - (KEEP - (TAPS - 1))
            if 0 <= tap < TAPS:
                acc = acc + par[tap : tap + 1, lanes] * shifted[base : base + rows]
    return acc


def conv_rest_kernel(*refs, n, m, tables, layer):
    at, glu_a, glu_b = refs[:3]
    par_a, par_b = refs[3].at[layer], refs[4].at[layer]
    wa, wb = refs[5 : 5 + n], refs[5 + n : 5 + n + m]
    mixed, t1, t2, wo, win = refs[5 + n + m :]

    def block(r, _):
        here = pl.multiple_of(r * ROWS, KEEP)
        s1 = jnp.zeros((REST, 128), F32)
        s2 = jnp.zeros((REST, 128), F32)
        for strip in range(4):
            lanes = slice((strip % 2) * 128, (strip % 2) * 128 + 128)
            glu, par = (glu_a, par_a) if strip < 2 else (glu_b, par_b)
            win[...] = glu[pl.ds(here, ROWS), lanes].astype(F32)
            acc = conv_strip(win, par, lanes, REST)
            mixed[pl.ds(pl.multiple_of(r * REST, REST), REST), strip * 128 : strip * 128 + 128] = acc
            s1 = s1 + acc
            s2 = s2 + acc * acc
        t1[pl.ds(pl.multiple_of(r * REST, REST), REST)] = s1
        t2[pl.ds(pl.multiple_of(r * REST, REST), REST)] = s2
        return 0

    lax.fori_loop(0, 4, block, 0)
    spread(at, wa, tables[0], wo, slice(2 * CH, 3 * CH), slice(0, CH))
    spread(at, wb, tables[1], wo, slice(2 * CH, 3 * CH), slice(CH, 2 * CH))


def conv_edge_kernel(at, glu_a, glu_b, other, before, par_a, par_b, t1, t2, mixed, stats, win, l1, l2, *, layer):
    par_a, par_b = par_a.at[layer], par_b.at[layer]
    x, c = at[2], at[3]

    def block(r, _):
        idx = jnp.where(c == 1, r, (r + 1) % 4)
        first = jnp.logical_and(c == 0, r == x)
        here = pl.multiple_of(r * ROWS, KEEP)
        edge_at = pl.multiple_of(idx * KEEP, KEEP)
        s1 = jnp.zeros((KEEP, 128), F32)
        s2 = jnp.zeros((KEEP, 128), F32)
        for strip in range(4):
            lanes = slice((strip % 2) * 128, (strip % 2) * 128 + 128)
            there = slice(((strip + 2) % 4) * 128, ((strip + 2) % 4) * 128 + 128)
            glu, par = (glu_a, par_a) if strip < 2 else (glu_b, par_b)
            edge = other[pl.ds(edge_at, KEEP), there].astype(F32)
            win[0:KEEP] = jnp.where(first, before[:, there].astype(F32), edge)
            win[KEEP:] = glu[pl.ds(here, KEEP), lanes].astype(F32)
            acc = conv_strip(win, par, lanes, KEEP)
            mixed[pl.ds(pl.multiple_of(r * KEEP, KEEP), KEEP), strip * 128 : strip * 128 + 128] = acc
            s1 = s1 + acc
            s2 = s2 + acc * acc
        l1[pl.ds(pl.multiple_of(r * KEEP, KEEP), KEEP)] = s1
        l2[pl.ds(pl.multiple_of(r * KEEP, KEEP), KEEP)] = s2
        return 0

    lax.fori_loop(0, 4, block, 0)
    for o, low, high in ((0, l1, t1), (4, l2, t2)):
        for r in range(4):
            rows = [low[r * KEEP : (r + 1) * KEEP], high[r * REST : (r + 1) * REST]]
            rows = jnp.concatenate(rows + [jnp.zeros((128 - ROWS, 128), F32)], axis=0)
            stats[o + r : o + r + 1] = jnp.sum(rows.T, axis=0, keepdims=True)


def out_kernel(*refs, blocks, layer):
    at, low, high, stats, par_a, par_b, wo = refs[:7]
    outs, act = refs[7:-1], refs[-1]
    par_a, par_b = par_a.at[layer], par_b.at[layer]
    x = at[2]
    own, m, f, p = (stats[pl.ds(pl.multiple_of(((x + d) % 4) * 8, 8), 8)] for d in (0, 3, 2, 1))
    rows = []
    for o in (0, 4):
        for r in range(4):
            i, j, k = o + (r - 1) % 4, o + (r + 2) % 4, o + (r + 1) % 4
            rows.append(own[o + r : o + r + 1] + m[i : i + 1] + f[j : j + 1] + p[k : k + 1])
    mean = jnp.concatenate(rows[:4], axis=0) * (1.0 / CHANNELS)
    msq = jnp.concatenate(rows[4:], axis=0) * (1.0 / CHANNELS)
    inv = lax.rsqrt(msq - mean * mean + EPS)
    cols = jnp.concatenate([mean, inv], axis=0).T
    for n, r in enumerate(blocks):
        for src, size, first in ((low, KEEP, 0), (high, REST, KEEP)):
            mu = cols[first : first + size, r : r + 1]
            iv = cols[first : first + size, 4 + r : 5 + r]
            for s, par in ((0, par_a), (1, par_b)):
                v = (src[r * size : (r + 1) * size, s * CH : (s + 1) * CH] - mu) * iv
                v = v * par[TAPS + 1 : TAPS + 2] + par[TAPS + 2 : TAPS + 3]
                to = n * ROWS + first
                act[to : to + size, s * CH : (s + 1) * CH] = (v / (1.0 + jnp.exp(-v))).astype(BF)
    d = lax.dot_general(act[...], wo[...], (((1,), (1,)), ((), ())), preferred_element_type=F32)
    for n, out in enumerate(outs):
        out[...] = d[n * ROWS : (n + 1) * ROWS].astype(out.dtype)


def add_kernel(at, h, o0, m, p, f, out, *, last):
    for k in range(8):
        src = slice(k * CH, (k + 1) * CH)
        t = o0[:, src] + m[:, src].astype(F32) + p[:, src].astype(F32) + f[:, src].astype(F32)
        t = (h[:, src].astype(F32) + t).astype(BF)
        if last:
            out[:, pl.ds(pl.multiple_of(((at[0] + k) % 8) * CH, CH), CH)] = t
        else:
            out[:, src] = t


def out_call(layer, blocks, kinds, *inputs):
    return call(
        functools.partial(out_kernel, blocks=blocks, layer=layer),
        [((ROWS, WIDTH), k) for k in kinds],
        list(inputs),
        [pltpu.VMEM((len(blocks) * ROWS, 2 * CH), BF)],
    )


def layer_body(layer, at, state, tokens, own, other, par, before_pairs):
    glu_a, glu_b, tails, last = glu_calls(at, tokens, own, other)
    there = swap(tails)
    before = lax.ppermute(last, ("z", "y", "c"), before_pairs)
    par_a, par_b = par
    (a, ta), (b, tb) = own, other
    high, t1, t2, wo = call(
        functools.partial(conv_rest_kernel, n=len(a), m=len(b), tables=(ta, tb), layer=layer),
        [((4 * REST, 2 * CH), F32)] + [((4 * REST, 128), F32)] * 2 + [((WIDTH, 2 * CH), BF)],
        [at, glu_a, glu_b, par_a, par_b, *a, *b],
        [pltpu.VMEM((ROWS, 128), F32)],
    )
    low, s = call(
        functools.partial(conv_edge_kernel, layer=layer),
        [((4 * KEEP, 2 * CH), F32), ((8, 128), F32)],
        [at, glu_a, glu_b, there, before, par_a, par_b, t1, t2],
        [pltpu.VMEM((2 * KEEP, 128), F32)] + [pltpu.VMEM((4 * KEEP, 128), F32)] * 2,
    )
    stats = lax.all_to_all(jnp.broadcast_to(s[None], (4, 8, 128)), "x", 0, 0, tiled=True)
    inputs = (at, low, high, stats.reshape(32, 128), par_a, par_b, wo)
    (o2,) = out_call(layer, (2,), (BF,), *inputs)
    from_f = take(o2, "x", 2)
    o3, o1, o0 = out_call(layer, (3, 1, 0), (BF, BF, F32), *inputs)
    from_m, from_p = take(o3, "x", -1), take(o1, "x", 1)
    (state,) = call(
        functools.partial(add_kernel, last=layer == 1),
        [((ROWS, WIDTH), BF)],
        [at, state, o0, from_m, from_p, from_f],
    )
    return state, o1


def gather_tokens(h):
    m, p, f = take(h, "x", -1), take(h, "x", 1), take(h, "x", 2)
    return h, m, f, p


def body(hidden, norm_gain, w_value, w_gate, conv_weight, conv_bias, chan_gain, chan_shift, w_out):
    z, y, x, c = (lax.axis_index(a) for a in SP_TP)
    at = jnp.stack([z, y, x, c]).astype(jnp.int32)
    b0, b1 = call(
        fold_kernel,
        [((PIECE, BUNDLE), BF)] * 2,
        [at, norm_gain, w_value, w_gate, w_out.swapaxes(1, 2)],
        [pltpu.VMEM((128, 128), F32)],
    )
    (state,) = call(roll_kernel, [((ROWS, WIDTH), BF)], [at, hidden])
    (small,) = call(
        par_kernel,
        [((2, 40, CH), F32)],
        [conv_weight.swapaxes(0, 1), conv_bias, chan_gain, chan_shift],
        scalars=False,
    )

    za, zb, z4 = take(b0, "z", 1), take(b0, "z", -1), take(b0, "z", 4)
    z2 = take(jnp.concatenate([b0, za], axis=0), "z", 2)
    z6 = take(jnp.concatenate([b0, zb], axis=0), "z", -2)
    size, cut = 8 * PIECE, 4 * PIECE
    (line,) = call(line_kernel, [((size, BUNDLE), BF)], [b0, za, zb, z2, z4, z6], scalars=False)
    up, down = take(line, "y", 1), take(line, "y", -1)
    fu, fd = take(up[:cut], "y", 1), take(down[cut:], "y", -1)
    s2 = swap(jnp.concatenate([line, up, down], axis=0))
    s3 = swap(jnp.concatenate([fu, fd], axis=0))
    own0 = (
        [line, up, down, fu, fd],
        [(0, 0, (0, 0), size), (1, 0, (1, 0), size), (2, 0, (3, 0), size)]
        + [(3, 0, (2, 0), cut), (4, 0, (2, 4), cut)],
    )
    other0 = (
        [s2, s3],
        [(0, n * size, (dy, 0), size) for n, dy in enumerate((0, 1, 3))]
        + [(1, 0, (2, 0), size)],
    )

    g = [b1, take(b1, "y", 1), take(b1, "y", 2), take(b1, "y", 3)]
    (near,) = call(near_kernel, [((CH, BUNDLE), BF)], [at, *g])
    p1, m1 = take(near, "z", 1), take(near, "z", -1)
    p2, m2 = take(p1, "z", 1), take(m1, "z", -1)
    p3, m3 = take(p2, "z", 1), take(m2, "z", -1)
    p4 = take(p3, "z", 1)
    chunks = [near, p1, p2, p3, p4, m3, m2, m1]

    par = (small, swap(small))
    size = lax.axis_size("z") * lax.axis_size("y")
    pairs = [(2 * i + 1, 2 * (i + 1)) for i in range(size - 1)]
    state, ready = layer_body(0, at, state, gather_tokens(state), own0, other0, par, pairs)
    (both,) = call(cat_kernel, [((WIDTH, BUNDLE), BF)], [*chunks, ready], scalars=False)
    ysw = swap(both)
    own1 = (chunks, [(k, 0, k * CH, CH) for k in range(8)])
    other1 = ([ysw], [(0, 0, 0, WIDTH)])
    state, _ = layer_body(1, at, state, gather_tokens(state), own1, other1, par, pairs)
    return state


def solution(mesh):
    torus = Mesh(mesh.devices.reshape(8, 4, 4, 2), SP_TP)
    tp = ("x", "c")
    in_specs = (
        P(SP_TP, None),
        P(),
        P(None, SP, tp),
        P(None, SP, tp),
        P(None, None, tp),
        P(None, tp),
        P(None, tp),
        P(None, tp),
        P(None, tp, SP),
    )
    return jax.shard_map(
        body, mesh=torus, in_specs=in_specs, out_specs=P(SP_TP, None), check_vma=False
    )
```

profile of v0, /device:TPU:1, one launch (start us, length us, event | category | flops | bytes accessed | tf_op | source)
XLA Modules:
  0.0 206.4 jit_solution(7991530055030940552)
XLA Ops:
  4.1 6.5 %collective-permute-start.3 = (bf16[64,768]{1,0:T(8,128)(2,1)S(1)}, bf16[64,768]{1,0:T(8,128)(2,1)S(1)}, u32[]{:S(2)}, u32[]{:S(2)}) collective-permute-start(bf16[64,768]{1,0:T(8,128)(2,1)S(1)} %get-tuple-element.37.own), channel_id=1, source_target_pairs={{32,0},{64,32},{96,64},{128,96},{160,128},{192,160},{224,192},{0,2... | collective-permute-start | bytes 294920 | tf_op jit(solution)/shard_map/ppermute | solution.py:30
  10.5 1.6 collective-permute-done.3.za
  12.2 3.0 %collective-permute-done.4.zb = bf16[64,768]{1,0:T(8,128)(2,1)S(1)} collective-permute-done((bf16[64,768]{1,0:T(8,128)(2,1)S(1)}, bf16[64,768]{1,0:T(8,128)(2,1)S(1)}, u32[]{:S(2)}, u32[]{:S(2)}) %collective-permute-start.4) | collective-permute-done | bytes 98336 | tf_op jit(solution)/shard_map/ppermute | solution.py:30
  15.6 2.1 %collective-permute-start.7 = (bf16[128,768]{1,0:T(8,128)(2,1)S(1)}, bf16[128,768]{1,0:T(8,128)(2,1)S(1)}, u32[]{:S(2)}, u32[]{:S(2)}) collective-permute-start(bf16[128,768]{1,0:T(8,128)(2,1)S(1)} %get-tuple-element.69), channel_id=1, source_target_pairs={{192,0},{224,32},{0,64},{32,96},{64,128},{96,160},{128,192},{160,2... | collective-permute-start | bytes 589832 | tf_op jit(solution)/shard_map/ppermute | solution.py:30
  17.7 1.4 collective-permute-start.6
  19.1 10.2 %collective-permute-done.6.z4 = bf16[64,768]{1,0:T(8,128)(2,1)S(1)} collective-permute-done((bf16[64,768]{1,0:T(8,128)(2,1)S(1)}, bf16[64,768]{1,0:T(8,128)(2,1)S(1)}, u32[]{:S(2)}, u32[]{:S(2)}) %collective-permute-start.6) | collective-permute-done | bytes 98336 | tf_op jit(solution)/shard_map/ppermute | solution.py:30
  30.2 2.8 %collective-permute-start.8 = (bf16[512,768]{1,0:T(8,128)(2,1)S(1)}, bf16[512,768]{1,0:T(8,128)(2,1)S(1)}, u32[]{:S(2)}, u32[]{:S(2)}) collective-permute-start(bf16[512,768]{1,0:T(8,128)(2,1)S(1)} %shard_map.93.refs_5_), channel_id=1, source_target_pairs={{8,0},{16,8},{24,16},{0,24},{9,1},{17,9},{25,17},{1,25},{10,2},{18... | collective-permute-start | bytes 2359304 | tf_op jit(solution)/shard_map/ppermute | solution.py:30
  33.0 15.2 %collective-permute-done.8.refs_6_ = bf16[512,768]{1,0:T(8,128)(2,1)S(1)} collective-permute-done((bf16[512,768]{1,0:T(8,128)(2,1)S(1)}, bf16[512,768]{1,0:T(8,128)(2,1)S(1)}, u32[]{:S(2)}, u32[]{:S(2)}) %collective-permute-start.8) | collective-permute-done | bytes 786464 | tf_op jit(solution)/shard_map/ppermute | solution.py:30
  48.1 3.1 %collective-permute-done.9.refs_7_ = bf16[512,768]{1,0:T(8,128)(2,1)S(1)} collective-permute-done((bf16[512,768]{1,0:T(8,128)(2,1)S(1)}, bf16[512,768]{1,0:T(8,128)(2,1)S(1)}, u32[]{:S(2)}, u32[]{:S(2)}) %collective-permute-start.9) | collective-permute-done | bytes 786464 | tf_op jit(solution)/shard_map/ppermute | solution.py:30
  51.4 3.0 %collective-permute-start.12 = (bf16[1536,768]{1,0:T(8,128)(2,1)S(1)}, bf16[1536,768]{1,0:T(8,128)(2,1)S(1)}, u32[]{:S(2)}, u32[]{:S(2)}) collective-permute-start(bf16[1536,768]{1,0:T(8,128)(2,1)S(1)} %pad_maximum_fusion), channel_id=1, source_target_pairs={{0,1},{1,0},{2,3},{3,2},{4,5},{5,4},{6,7},{7,6},{8,9},{9,8},{10,11... | collective-permute-start | bytes 7077896 | tf_op jit(solution)/shard_map/ppermute | solution.py:34
  55.9 2.8 %collective-permute-done.23.a1 = bf16[64,768]{1,0:T(8,128)(2,1)S(1)} collective-permute-done((bf16[64,768]{1,0:T(8,128)(2,1)S(1)}, bf16[64,768]{1,0:T(8,128)(2,1)S(1)}, u32[]{:S(2)}, u32[]{:S(2)}) %collective-permute-start.23) | collective-permute-done | bytes 98336 | tf_op jit(solution)/shard_map/ppermute | solution.py:30
  59.9 2.9 %collective-permute-done.25.a3 = bf16[64,768]{1,0:T(8,128)(2,1)S(1)} collective-permute-done((bf16[64,768]{1,0:T(8,128)(2,1)S(1)}, bf16[64,768]{1,0:T(8,128)(2,1)S(1)}, u32[]{:S(2)}, u32[]{:S(2)}) %collective-permute-start.25) | collective-permute-done | bytes 98336 | tf_op jit(solution)/shard_map/ppermute | solution.py:30
  65.7 1.3 collective-permute-start
  67.0 6.6 %collective-permute-done.26.refs_6_.refs_1_ = bf16[256,768]{1,0:T(8,128)(2,1)S(1)} collective-permute-done((bf16[256,768]{1,0:T(8,128)(2,1)S(1)}, bf16[256,768]{1,0:T(8,128)(2,1)S(1)}, u32[]{:S(2)}, u32[]{:S(2)}) %collective-permute-start.26) | collective-permute-done | bytes 393248 | tf_op jit(solution)/shard_map/ppermute | solution.py:30
  74.8 1.6 collective-permute-start.27
  76.4 2.7 %collective-permute-start.1 = (bf16[96,2048]{1,0:T(8,128)(2,1)S(1)}, bf16[96,2048]{1,0:T(8,128)(2,1)S(1)}, u32[]{:S(2)}, u32[]{:S(2)}) collective-permute-start(bf16[96,2048]{1,0:T(8,128)(2,1)S(1)} %shard_map.91.refs_1_.h), channel_id=1, source_target_pairs={{4,0},{6,2},{0,4},{2,6},{5,1},{7,3},{1,5},{3,7},{12,8},{14,10},{8,... | collective-permute-start | bytes 1179656 | tf_op jit(solution)/shard_map/ppermute | solution.py:30
  79.3 2.3 %collective-permute-start.13 = (bf16[512,768]{1,0:T(8,128)(2,1)S(1)}, bf16[512,768]{1,0:T(8,128)(2,1)S(1)}, u32[]{:S(2)}, u32[]{:S(2)}) collective-permute-start(bf16[512,768]{1,0:T(8,128)(2,1)S(1)} %pad_maximum_fusion.1), channel_id=1, source_target_pairs={{0,1},{1,0},{2,3},{3,2},{4,5},{5,4},{6,7},{7,6},{8,9},{9,8},{10,11... | collective-permute-start | bytes 2359304 | tf_op jit(solution)/shard_map/ppermute | solution.py:34
  81.5 2.6 %collective-permute-done.30.refs_12_.refs_7_ = bf16[256,768]{1,0:T(8,128)(2,1)S(1)} collective-permute-done((bf16[256,768]{1,0:T(8,128)(2,1)S(1)}, bf16[256,768]{1,0:T(8,128)(2,1)S(1)}, u32[]{:S(2)}, u32[]{:S(2)}) %collective-permute-start.30) | collective-permute-done | bytes 393248 | tf_op jit(solution)/shard_map/ppermute | solution.py:30
  84.5 2.4 %collective-permute-start.28 = (bf16[256,768]{1,0:T(8,128)(2,1)S(1)}, bf16[256,768]{1,0:T(8,128)(2,1)S(1)}, u32[]{:S(2)}, u32[]{:S(2)}) collective-permute-start(bf16[256,768]{1,0:T(8,128)(2,1)S(1)} %collective-permute-done.27.refs_7_.refs_2_), channel_id=1, source_target_pairs={{32,0},{64,32},{96,64},{128,96},{160,128},{192,160},{224,192},{0,2... | collective-permute-start | bytes 1179656 | tf_op jit(solution)/shard_map/ppermute | solution.py:30
  86.8 2.5 %collective-permute-start.2 = (bf16[96,2048]{1,0:T(8,128)(2,1)S(1)}, bf16[96,2048]{1,0:T(8,128)(2,1)S(1)}, u32[]{:S(2)}, u32[]{:S(2)}) collective-permute-start(bf16[96,2048]{1,0:T(8,128)(2,1)S(1)} %shard_map.91.refs_1_.h), channel_id=1, source_target_pairs={{2,0},{4,2},{6,4},{0,6},{3,1},{5,3},{7,5},{1,7},{10,8},{12,10},{14... | collective-permute-start | bytes 1179656 | tf_op jit(solution)/shard_map/ppermute | solution.py:30
  89.3 4.5 %collective-permute-done.31.refs_11_.refs_6_ = bf16[256,768]{1,0:T(8,128)(2,1)S(1)} collective-permute-done((bf16[256,768]{1,0:T(8,128)(2,1)S(1)}, bf16[256,768]{1,0:T(8,128)(2,1)S(1)}, u32[]{:S(2)}, u32[]{:S(2)}) %collective-permute-start.31) | collective-permute-done | bytes 393248 | tf_op jit(solution)/shard_map/ppermute | solution.py:30
  93.9 2.7 %collective-permute-start.29 = (bf16[256,768]{1,0:T(8,128)(2,1)S(1)}, bf16[256,768]{1,0:T(8,128)(2,1)S(1)}, u32[]{:S(2)}, u32[]{:S(2)}) collective-permute-start(bf16[256,768]{1,0:T(8,128)(2,1)S(1)} %collective-permute-done.28.refs_8_.refs_3_), channel_id=1, source_target_pairs={{32,0},{64,32},{96,64},{128,96},{160,128},{192,160},{224,192},{0,2... | collective-permute-start | bytes 1179656 | tf_op jit(solution)/shard_map/ppermute | solution.py:30
  96.5 2.3 %shard_map.94 = (bf16[384,256]{1,0:T(8,128)(2,1)S(1)}, bf16[384,2048]{1,0:T(8,128)(2,1)S(1)}, f32[384,128]{1,0:T(8,128)S(1)}) custom-call(s32[4]{0:T(128)S(1)} %pad_add_fusion.at.refs_0_, bf16[96,2048]{1,0:T(8,128)(2,1)S(1)} %shard_map.91.refs_1_.h, bf16[96,2048]{1,0:T(8,128)(2,1)S(1)} %collective-permute-done.refs_2_, ...), custom_call_target="tpu_custom_call" | custom-call | tf_op jit(solution)/shard_map/pallas_call | solution.py:41
  98.9 1.8 shard_map.95
  100.7 3.7 %collective-permute-start.14 = (bf16[128,512]{1,0:T(8,128)(2,1)S(1)}, bf16[128,512]{1,0:T(8,128)(2,1)S(1)}, u32[]{:S(2)}, u32[]{:S(2)}) collective-permute-start(bf16[128,512]{1,0:T(8,128)(2,1)S(1)} %get-tuple-element.42), channel_id=1, source_target_pairs={{0,1},{1,0},{2,3},{3,2},{4,5},{5,4},{6,7},{7,6},{8,9},{9,8},{10,11... | collective-permute-start | bytes 393224 | tf_op jit(solution)/shard_map/ppermute | solution.py:34
  105.9 2.3 %shard_map.97 = (f32[256,512]{1,0:T(8,128)S(1)}, f32[256,128]{1,0:T(8,128)S(1)}, f32[256,128]{1,0:T(8,128)S(1)}, bf16[2048,512]{1,0:T(8,128)(2,1)S(1)}) custom-call(s32[4]{0:T(128)S(1)} %pad_add_fusion.at.refs_0_, bf16[384,256]{1,0:T(8,128)(2,1)S(1)} %get-tuple-element.38.refs_3_.refs_1_.glu_a, bf16[384,256]{1,0:T(8,128)(2,1)S(1)} %get-tuple-element.41.refs_2_.glu_b, ...), custom_call_target="tpu_custom_call" | custom-call | tf_op jit(solution)/shard_map/pallas_call | solution.py:41
  108.2 1.4 shard_map.98
  109.7 8.0 %all_to_all.10 = f32[4,8,128]{2,1,0:T(8,128)S(1)} all-to-all(f32[4,8,128]{2,1,0:T(8,128)S(1)} %broadcast_in_dim.4), channel_id=1, replica_groups=mesh['z'=8,'y'=4,'x'=4,'c'=2] {'x'}, dimensions={0} | all-to-all | bytes 32768 | tf_op jit(solution)/shard_map/all_to_all | solution.py:302
  117.7 1.6 shard_map.99
  119.6 1.6 collective-permute-start.33
  122.7 1.4 shard_map.100
  125.0 17.0 %collective-permute-done.17.m = bf16[96,2048]{1,0:T(8,128)(2,1)S(1)} collective-permute-done((bf16[96,2048]{1,0:T(8,128)(2,1)S(1)}, bf16[96,2048]{1,0:T(8,128)(2,1)S(1)}, u32[]{:S(2)}, u32[]{:S(2)}) %collective-permute-start.17) | collective-permute-done | bytes 393248 | tf_op jit(solution)/shard_map/ppermute | solution.py:30
  142.9 1.7 collective-permute-start.21
  145.8 8.4 %collective-permute-done.20.refs_2_ = bf16[96,2048]{1,0:T(8,128)(2,1)S(1)} collective-permute-done((bf16[96,2048]{1,0:T(8,128)(2,1)S(1)}, bf16[96,2048]{1,0:T(8,128)(2,1)S(1)}, u32[]{:S(2)}, u32[]{:S(2)}) %collective-permute-start.20) | collective-permute-done | bytes 393248 | tf_op jit(solution)/shard_map/ppermute | solution.py:30
  154.2 7.2 %collective-permute-done.21.refs_3_ = bf16[96,2048]{1,0:T(8,128)(2,1)S(1)} collective-permute-done((bf16[96,2048]{1,0:T(8,128)(2,1)S(1)}, bf16[96,2048]{1,0:T(8,128)(2,1)S(1)}, u32[]{:S(2)}, u32[]{:S(2)}) %collective-permute-start.21) | collective-permute-done | bytes 393248 | tf_op jit(solution)/shard_map/ppermute | solution.py:30
  161.4 1.7 collective-permute-done.22.refs_4_
  163.1 2.2 %shard_map.103 = (bf16[384,256]{1,0:T(8,128)(2,1)S(1)}, bf16[384,2048]{1,0:T(8,128)(2,1)S(1)}, f32[384,128]{1,0:T(8,128)S(1)}) custom-call(s32[4]{0:T(128)S(1)} %pad_add_fusion.at.refs_0_, bf16[96,2048]{1,0:T(8,128)(2,1)S(1)} %shard_map.101.refs_1_.h, bf16[96,2048]{1,0:T(8,128)(2,1)S(1)} %collective-permute-done.20.refs_2_, ...), custom_call_target="tpu_custom_call" | custom-call | tf_op jit(solution)/shard_map/pallas_call | solution.py:41
  165.3 1.8 shard_map.105
  167.1 1.7 collective-permute-start.34
  168.8 2.8 %collective-permute-start.35 = (bf16[32,512]{1,0:T(8,128)(2,1)S(1)}, bf16[32,512]{1,0:T(8,128)(2,1)S(1)}, u32[]{:S(2)}, u32[]{:S(2)}) collective-permute-start(bf16[32,512]{1,0:T(8,128)(2,1)S(1)} %get-tuple-element.59), channel_id=1, source_target_pairs={{1,8},{9,16},{17,24},{25,32},{33,40},{41,48},{49,56},{57,64},{65,7... | collective-permute-start | bytes 98312 | tf_op jit(solution)/shard_map/ppermute | solution.py:287
  171.6 2.1 %shard_map.106 = (f32[256,512]{1,0:T(8,128)S(1)}, f32[256,128]{1,0:T(8,128)S(1)}, f32[256,128]{1,0:T(8,128)S(1)}, bf16[2048,512]{1,0:T(8,128)(2,1)S(1)}) custom-call(s32[4]{0:T(128)S(1)} %pad_add_fusion.at.refs_0_, bf16[384,256]{1,0:T(8,128)(2,1)S(1)} %get-tuple-element.54.refs_3_.refs_1_.glu_a, bf16[384,256]{1,0:T(8,128)(2,1)S(1)} %get-tuple-element.57.refs_2_.glu_b, ...), custom_call_target="tpu_custom_call" | custom-call | tf_op jit(solution)/shard_map/pallas_call | solution.py:41
  173.7 1.4 shard_map.107
  175.2 7.6 %all_to_all.11 = f32[4,8,128]{2,1,0:T(8,128)S(1)} all-to-all(f32[4,8,128]{2,1,0:T(8,128)S(1)} %broadcast_in_dim.5), channel_id=1, replica_groups=mesh['z'=8,'y'=4,'x'=4,'c'=2] {'x'}, dimensions={0} | all-to-all | bytes 32768 | tf_op jit(solution)/shard_map/all_to_all | solution.py:302
  182.8 1.6 shard_map.108
  184.8 2.4 %collective-permute-start.37 = (bf16[96,2048]{1,0:T(8,128)(2,1)S(1)}, bf16[96,2048]{1,0:T(8,128)(2,1)S(1)}, u32[]{:S(2)}, u32[]{:S(2)}) collective-permute-start(bf16[96,2048]{1,0:T(8,128)(2,1)S(1)} %get-tuple-element.68), channel_id=1, source_target_pairs={{2,0},{4,2},{6,4},{0,6},{3,1},{5,3},{7,5},{1,7},{10,8},{12,10},{14... | collective-permute-start | bytes 1179656 | tf_op jit(solution)/shard_map/ppermute | solution.py:30
  187.2 1.4 shard_map.109
  188.7 16.2 %collective-permute-done.36.m = bf16[96,2048]{1,0:T(8,128)(2,1)S(1)} collective-permute-done((bf16[96,2048]{1,0:T(8,128)(2,1)S(1)}, bf16[96,2048]{1,0:T(8,128)(2,1)S(1)}, u32[]{:S(2)}, u32[]{:S(2)}) %collective-permute-start.36) | collective-permute-done | bytes 393248 | tf_op jit(solution)/shard_map/ppermute | solution.py:30
  204.9 1.5 shard_map.110
  (78 shorter events, 19.2 us)
Async XLA Ops:
  0.1 0.8 copy-start.1
  0.9 0.8 copy-start.2
  1.8 0.8 copy-start.3
  2.6 0.7 copy-start.5
  4.1 8.1 %collective-permute-start.3 = (bf16[64,768]{1,0:T(8,128)(2,1)S(1)}, bf16[64,768]{1,0:T(8,128)(2,1)S(1)}, u32[]{:S(2)}, u32[]{:S(2)}) collective-permute-start(bf16[64,768]{1,0:T(8,128)(2,1)S(1)} %get-tuple-element.37.own), channel_id=1, source_target_pairs={{32,0},{64,32},{96,64},{128,96},{160,128},{192,160},{224,192},{0,2... | collective-permute-start | bytes 294920 | tf_op jit(solution)/shard_map/ppermute | solution.py:30
  10.5 4.7 %collective-permute-start.4 = (bf16[64,768]{1,0:T(8,128)(2,1)S(1)}, bf16[64,768]{1,0:T(8,128)(2,1)S(1)}, u32[]{:S(2)}, u32[]{:S(2)}) collective-permute-start(bf16[64,768]{1,0:T(8,128)(2,1)S(1)} %get-tuple-element.37.own), channel_id=1, source_target_pairs={{224,0},{0,32},{32,64},{64,96},{96,128},{128,160},{160,192},{192,2... | collective-permute-start | bytes 294920 | tf_op jit(solution)/shard_map/ppermute | solution.py:30
  15.2 14.8 %collective-permute-start.5 = (bf16[128,768]{1,0:T(8,128)(2,1)S(1)}, bf16[128,768]{1,0:T(8,128)(2,1)S(1)}, u32[]{:S(2)}, u32[]{:S(2)}) collective-permute-start(bf16[128,768]{1,0:T(8,128)(2,1)S(1)} %get-tuple-element.70), channel_id=1, source_target_pairs={{64,0},{96,32},{128,64},{160,96},{192,128},{224,160},{0,192},{32,2... | collective-permute-start | bytes 589832 | tf_op jit(solution)/shard_map/ppermute | solution.py:30
  15.6 14.5 %collective-permute-start.7 = (bf16[128,768]{1,0:T(8,128)(2,1)S(1)}, bf16[128,768]{1,0:T(8,128)(2,1)S(1)}, u32[]{:S(2)}, u32[]{:S(2)}) collective-permute-start(bf16[128,768]{1,0:T(8,128)(2,1)S(1)} %get-tuple-element.69), channel_id=1, source_target_pairs={{192,0},{224,32},{0,64},{32,96},{64,128},{96,160},{128,192},{160,2... | collective-permute-start | bytes 589832 | tf_op jit(solution)/shard_map/ppermute | solution.py:30
  17.7 11.7 %collective-permute-start.6 = (bf16[64,768]{1,0:T(8,128)(2,1)S(1)}, bf16[64,768]{1,0:T(8,128)(2,1)S(1)}, u32[]{:S(2)}, u32[]{:S(2)}) collective-permute-start(bf16[64,768]{1,0:T(8,128)(2,1)S(1)} %get-tuple-element.37.own), channel_id=1, source_target_pairs={{128,0},{160,32},{192,64},{224,96},{0,128},{32,160},{64,192},{96,2... | collective-permute-start | bytes 294920 | tf_op jit(solution)/shard_map/ppermute | solution.py:30
  30.2 18.0 %collective-permute-start.8 = (bf16[512,768]{1,0:T(8,128)(2,1)S(1)}, bf16[512,768]{1,0:T(8,128)(2,1)S(1)}, u32[]{:S(2)}, u32[]{:S(2)}) collective-permute-start(bf16[512,768]{1,0:T(8,128)(2,1)S(1)} %shard_map.93.refs_5_), channel_id=1, source_target_pairs={{8,0},{16,8},{24,16},{0,24},{9,1},{17,9},{25,17},{1,25},{10,2},{18... | collective-permute-start | bytes 2359304 | tf_op jit(solution)/shard_map/ppermute | solution.py:30
  33.0 18.3 %collective-permute-start.9 = (bf16[512,768]{1,0:T(8,128)(2,1)S(1)}, bf16[512,768]{1,0:T(8,128)(2,1)S(1)}, u32[]{:S(2)}, u32[]{:S(2)}) collective-permute-start(bf16[512,768]{1,0:T(8,128)(2,1)S(1)} %shard_map.93.refs_5_), channel_id=1, source_target_pairs={{24,0},{0,8},{8,16},{16,24},{25,1},{1,9},{9,17},{17,25},{26,2},{2,... | collective-permute-start | bytes 2359304 | tf_op jit(solution)/shard_map/ppermute | solution.py:30
  51.4 13.7 %copy-start = (bf16[96,2048]{1,0:T(8,128)(2,1)S(1)}, bf16[96,2048]{1,0:T(8,128)(2,1)}, u32[]{:S(2)}) copy-start(bf16[96,2048]{1,0:T(8,128)(2,1)} %hidden.1) | copy-start | bytes 1179652
  51.4 47.4 %collective-permute-start.12 = (bf16[1536,768]{1,0:T(8,128)(2,1)S(1)}, bf16[1536,768]{1,0:T(8,128)(2,1)S(1)}, u32[]{:S(2)}, u32[]{:S(2)}) collective-permute-start(bf16[1536,768]{1,0:T(8,128)(2,1)S(1)} %pad_maximum_fusion), channel_id=1, source_target_pairs={{0,1},{1,0},{2,3},{3,2},{4,5},{5,4},{6,7},{7,6},{8,9},{9,8},{10,11... | collective-permute-start | bytes 7077896 | tf_op jit(solution)/shard_map/ppermute | solution.py:34
  54.4 4.3 %collective-permute-start.23 = (bf16[64,768]{1,0:T(8,128)(2,1)S(1)}, bf16[64,768]{1,0:T(8,128)(2,1)S(1)}, u32[]{:S(2)}, u32[]{:S(2)}) collective-permute-start(bf16[64,768]{1,0:T(8,128)(2,1)S(1)} %get-tuple-element.53.a0), channel_id=1, source_target_pairs={{8,0},{16,8},{24,16},{0,24},{9,1},{17,9},{25,17},{1,25},{10,2},{18... | collective-permute-start | bytes 294920 | tf_op jit(solution)/shard_map/ppermute | solution.py:30
  54.4 5.5 %collective-permute-start.24 = (bf16[64,768]{1,0:T(8,128)(2,1)S(1)}, bf16[64,768]{1,0:T(8,128)(2,1)S(1)}, u32[]{:S(2)}, u32[]{:S(2)}) collective-permute-start(bf16[64,768]{1,0:T(8,128)(2,1)S(1)} %get-tuple-element.53.a0), channel_id=1, source_target_pairs={{16,0},{24,8},{0,16},{8,24},{17,1},{25,9},{1,17},{9,25},{18,2},{26... | collective-permute-start | bytes 294920 | tf_op jit(solution)/shard_map/ppermute | solution.py:30
  55.0 7.8 %collective-permute-start.25 = (bf16[64,768]{1,0:T(8,128)(2,1)S(1)}, bf16[64,768]{1,0:T(8,128)(2,1)S(1)}, u32[]{:S(2)}, u32[]{:S(2)}) collective-permute-start(bf16[64,768]{1,0:T(8,128)(2,1)S(1)} %get-tuple-element.53.a0), channel_id=1, source_target_pairs={{24,0},{0,8},{8,16},{16,24},{25,1},{1,9},{9,17},{17,25},{26,2},{2,... | collective-permute-start | bytes 294920 | tf_op jit(solution)/shard_map/ppermute | solution.py:30
  63.3 10.3 %collective-permute-start.26 = (bf16[256,768]{1,0:T(8,128)(2,1)S(1)}, bf16[256,768]{1,0:T(8,128)(2,1)S(1)}, u32[]{:S(2)}, u32[]{:S(2)}) collective-permute-start(bf16[256,768]{1,0:T(8,128)(2,1)S(1)} %shard_map.102.refs_5_.refs_0_), channel_id=1, source_target_pairs={{32,0},{64,32},{96,64},{128,96},{160,128},{192,160},{224,192},{0,2... | collective-permute-start | bytes 1179656 | tf_op jit(solution)/shard_map/ppermute | solution.py:30
  63.4 11.4 %collective-permute-start.10 = (bf16[256,768]{1,0:T(8,128)(2,1)S(1)}, bf16[256,768]{1,0:T(8,128)(2,1)S(1)}, u32[]{:S(2)}, u32[]{:S(2)}) collective-permute-start(bf16[256,768]{1,0:T(8,128)(2,1)S(1)} %slice.8), channel_id=1, source_target_pairs={{8,0},{16,8},{24,16},{0,24},{9,1},{17,9},{25,17},{1,25},{10,2},{18... | collective-permute-start | bytes 1179656 | tf_op jit(solution)/shard_map/ppermute | solution.py:30
  64.0 12.5 %collective-permute-start.11 = (bf16[256,768]{1,0:T(8,128)(2,1)S(1)}, bf16[256,768]{1,0:T(8,128)(2,1)S(1)}, u32[]{:S(2)}, u32[]{:S(2)}) collective-permute-start(bf16[256,768]{1,0:T(8,128)(2,1)S(1)} %slice.9), channel_id=1, source_target_pairs={{24,0},{0,8},{8,16},{16,24},{25,1},{1,9},{9,17},{17,25},{26,2},{2,... | collective-permute-start | bytes 1179656 | tf_op jit(solution)/shard_map/ppermute | solution.py:30
  65.7 13.5 %collective-permute-start = (bf16[96,2048]{1,0:T(8,128)(2,1)S(1)}, bf16[96,2048]{1,0:T(8,128)(2,1)S(1)}, u32[]{:S(2)}, u32[]{:S(2)}) collective-permute-start(bf16[96,2048]{1,0:T(8,128)(2,1)S(1)} %shard_map.91.refs_1_.h), channel_id=1, source_target_pairs={{6,0},{0,2},{2,4},{4,6},{7,1},{1,3},{3,5},{5,7},{14,8},{8,10},{10,... | collective-permute-start | bytes 1179656 | tf_op jit(solution)/shard_map/ppermute | solution.py:30
  73.6 10.6 %collective-permute-start.30 = (bf16[256,768]{1,0:T(8,128)(2,1)S(1)}, bf16[256,768]{1,0:T(8,128)(2,1)S(1)}, u32[]{:S(2)}, u32[]{:S(2)}) collective-permute-start(bf16[256,768]{1,0:T(8,128)(2,1)S(1)} %shard_map.102.refs_5_.refs_0_), channel_id=1, source_target_pairs={{224,0},{0,32},{32,64},{64,96},{96,128},{128,160},{160,192},{192,2... | collective-permute-start | bytes 1179656 | tf_op jit(solution)/shard_map/ppermute | solution.py:30
  74.8 9.6 %collective-permute-start.27 = (bf16[256,768]{1,0:T(8,128)(2,1)S(1)}, bf16[256,768]{1,0:T(8,128)(2,1)S(1)}, u32[]{:S(2)}, u32[]{:S(2)}) collective-permute-start(bf16[256,768]{1,0:T(8,128)(2,1)S(1)} %collective-permute-done.26.refs_6_.refs_1_), channel_id=1, source_target_pairs={{32,0},{64,32},{96,64},{128,96},{160,128},{192,160},{224,192},{0,2... | collective-permute-start | bytes 1179656 | tf_op jit(solution)/shard_map/ppermute | solution.py:30
  76.4 10.4 %collective-permute-start.1 = (bf16[96,2048]{1,0:T(8,128)(2,1)S(1)}, bf16[96,2048]{1,0:T(8,128)(2,1)S(1)}, u32[]{:S(2)}, u32[]{:S(2)}) collective-permute-start(bf16[96,2048]{1,0:T(8,128)(2,1)S(1)} %shard_map.91.refs_1_.h), channel_id=1, source_target_pairs={{4,0},{6,2},{0,4},{2,6},{5,1},{7,3},{1,5},{3,7},{12,8},{14,10},{8,... | collective-permute-start | bytes 1179656 | tf_op jit(solution)/shard_map/ppermute | solution.py:30
  79.3 19.5 %collective-permute-start.13 = (bf16[512,768]{1,0:T(8,128)(2,1)S(1)}, bf16[512,768]{1,0:T(8,128)(2,1)S(1)}, u32[]{:S(2)}, u32[]{:S(2)}) collective-permute-start(bf16[512,768]{1,0:T(8,128)(2,1)S(1)} %pad_maximum_fusion.1), channel_id=1, source_target_pairs={{0,1},{1,0},{2,3},{3,2},{4,5},{5,4},{6,7},{7,6},{8,9},{9,8},{10,11... | collective-permute-start | bytes 2359304 | tf_op jit(solution)/shard_map/ppermute | solution.py:34
  84.1 9.7 %collective-permute-start.31 = (bf16[256,768]{1,0:T(8,128)(2,1)S(1)}, bf16[256,768]{1,0:T(8,128)(2,1)S(1)}, u32[]{:S(2)}, u32[]{:S(2)}) collective-permute-start(bf16[256,768]{1,0:T(8,128)(2,1)S(1)} %collective-permute-done.30.refs_12_.refs_7_), channel_id=1, source_target_pairs={{224,0},{0,32},{32,64},{64,96},{96,128},{128,160},{160,192},{192,2... | collective-permute-start | bytes 1179656 | tf_op jit(solution)/shard_map/ppermute | solution.py:30
  84.5 9.4 %collective-permute-start.28 = (bf16[256,768]{1,0:T(8,128)(2,1)S(1)}, bf16[256,768]{1,0:T(8,128)(2,1)S(1)}, u32[]{:S(2)}, u32[]{:S(2)}) collective-permute-start(bf16[256,768]{1,0:T(8,128)(2,1)S(1)} %collective-permute-done.27.refs_7_.refs_2_), channel_id=1, source_target_pairs={{32,0},{64,32},{96,64},{128,96},{160,128},{192,160},{224,192},{0,2... | collective-permute-start | bytes 1179656 | tf_op jit(solution)/shard_map/ppermute | solution.py:30
  86.8 9.7 %collective-permute-start.2 = (bf16[96,2048]{1,0:T(8,128)(2,1)S(1)}, bf16[96,2048]{1,0:T(8,128)(2,1)S(1)}, u32[]{:S(2)}, u32[]{:S(2)}) collective-permute-start(bf16[96,2048]{1,0:T(8,128)(2,1)S(1)} %shard_map.91.refs_1_.h), channel_id=1, source_target_pairs={{2,0},{4,2},{6,4},{0,6},{3,1},{5,3},{7,5},{1,7},{10,8},{12,10},{14... | collective-permute-start | bytes 1179656 | tf_op jit(solution)/shard_map/ppermute | solution.py:30
  93.8 25.5 %collective-permute-start.32 = (bf16[256,768]{1,0:T(8,128)(2,1)S(1)}, bf16[256,768]{1,0:T(8,128)(2,1)S(1)}, u32[]{:S(2)}, u32[]{:S(2)}) collective-permute-start(bf16[256,768]{1,0:T(8,128)(2,1)S(1)} %collective-permute-done.31.refs_11_.refs_6_), channel_id=1, source_target_pairs={{224,0},{0,32},{32,64},{64,96},{96,128},{128,160},{160,192},{192,2... | collective-permute-start | bytes 1179656 | tf_op jit(solution)/shard_map/ppermute | solution.py:30
  93.9 25.5 %collective-permute-start.29 = (bf16[256,768]{1,0:T(8,128)(2,1)S(1)}, bf16[256,768]{1,0:T(8,128)(2,1)S(1)}, u32[]{:S(2)}, u32[]{:S(2)}) collective-permute-start(bf16[256,768]{1,0:T(8,128)(2,1)S(1)} %collective-permute-done.28.refs_8_.refs_3_), channel_id=1, source_target_pairs={{32,0},{64,32},{96,64},{128,96},{160,128},{192,160},{224,192},{0,2... | collective-permute-start | bytes 1179656 | tf_op jit(solution)/shard_map/ppermute | solution.py:30
  98.8 5.6 %copy-start.4 = (f32[2,31,256]{2,0,1:T(2,128)S(1)}, f32[2,31,256]{2,0,1:T(2,128)}, u32[]{:S(2)}) copy-start(f32[2,31,256]{2,0,1:T(2,128)} %param.13) | copy-start | bytes 190468
  98.8 5.6 %copy-start.6 = (f32[2,256]{1,0:T(2,128)S(1)}, f32[2,256]{1,0:T(2,128)}, u32[]{:S(2)}) copy-start(f32[2,256]{1,0:T(2,128)} %cb.1) | copy-start | bytes 6148
  98.8 5.6 %copy-start.7 = (f32[2,256]{1,0:T(2,128)S(1)}, f32[2,256]{1,0:T(2,128)}, u32[]{:S(2)}) copy-start(f32[2,256]{1,0:T(2,128)} %cg.1) | copy-start | bytes 6148
  98.9 5.6 %copy-start.8 = (f32[2,256]{1,0:T(2,128)S(1)}, f32[2,256]{1,0:T(2,128)}, u32[]{:S(2)}) copy-start(f32[2,256]{1,0:T(2,128)} %cs.1) | copy-start | bytes 6148
  100.7 7.5 %collective-permute-start.14 = (bf16[128,512]{1,0:T(8,128)(2,1)S(1)}, bf16[128,512]{1,0:T(8,128)(2,1)S(1)}, u32[]{:S(2)}, u32[]{:S(2)}) collective-permute-start(bf16[128,512]{1,0:T(8,128)(2,1)S(1)} %get-tuple-element.42), channel_id=1, source_target_pairs={{0,1},{1,0},{2,3},{3,2},{4,5},{5,4},{6,7},{7,6},{8,9},{9,8},{10,11... | collective-permute-start | bytes 393224 | tf_op jit(solution)/shard_map/ppermute | solution.py:34
  104.5 1.4 collective-permute-start.16
  104.6 3.6 %collective-permute-start.15 = (bf16[32,512]{1,0:T(8,128)(2,1)S(1)}, bf16[32,512]{1,0:T(8,128)(2,1)S(1)}, u32[]{:S(2)}, u32[]{:S(2)}) collective-permute-start(bf16[32,512]{1,0:T(8,128)(2,1)S(1)} %get-tuple-element.43), channel_id=1, source_target_pairs={{1,8},{9,16},{17,24},{25,32},{33,40},{41,48},{49,56},{57,64},{65,7... | collective-permute-start | bytes 98312 | tf_op jit(solution)/shard_map/ppermute | solution.py:287
  119.6 45.7 %collective-permute-start.33 = (bf16[2048,768]{1,0:T(8,128)(2,1)S(1)}, bf16[2048,768]{1,0:T(8,128)(2,1)S(1)}, u32[]{:S(2)}, u32[]{:S(2)}) collective-permute-start(bf16[2048,768]{1,0:T(8,128)(2,1)S(1)} %shard_map.104), channel_id=1, source_target_pairs={{0,1},{1,0},{2,3},{3,2},{4,5},{5,4},{6,7},{7,6},{8,9},{9,8},{10,11... | collective-permute-start | bytes 9437192 | tf_op jit(solution)/shard_map/ppermute | solution.py:34
  121.2 20.8 %collective-permute-start.18 = (bf16[96,2048]{1,0:T(8,128)(2,1)S(1)}, bf16[96,2048]{1,0:T(8,128)(2,1)S(1)}, u32[]{:S(2)}, u32[]{:S(2)}) collective-permute-start(bf16[96,2048]{1,0:T(8,128)(2,1)S(1)} %get-tuple-element.52.refs_8_), channel_id=1, source_target_pairs={{2,0},{4,2},{6,4},{0,6},{3,1},{5,3},{7,5},{1,7},{10,8},{12,10},{14... | collective-permute-start | bytes 1179656 | tf_op jit(solution)/shard_map/ppermute | solution.py:30
  122.1 19.9 %collective-permute-start.17 = (bf16[96,2048]{1,0:T(8,128)(2,1)S(1)}, bf16[96,2048]{1,0:T(8,128)(2,1)S(1)}, u32[]{:S(2)}, u32[]{:S(2)}) collective-permute-start(bf16[96,2048]{1,0:T(8,128)(2,1)S(1)} %get-tuple-element.51), channel_id=1, source_target_pairs={{6,0},{0,2},{2,4},{4,6},{7,1},{1,3},{3,5},{5,7},{14,8},{8,10},{10,... | collective-permute-start | bytes 1179656 | tf_op jit(solution)/shard_map/ppermute | solution.py:30
  124.1 17.9 %collective-permute-start.19 = (bf16[96,2048]{1,0:T(8,128)(2,1)S(1)}, bf16[96,2048]{1,0:T(8,128)(2,1)S(1)}, u32[]{:S(2)}, u32[]{:S(2)}) collective-permute-start(bf16[96,2048]{1,0:T(8,128)(2,1)S(1)} %shard_map.100), channel_id=1, source_target_pairs={{4,0},{6,2},{0,4},{2,6},{5,1},{7,3},{1,5},{3,7},{12,8},{14,10},{8,... | collective-permute-start | bytes 1179656 | tf_op jit(solution)/shard_map/ppermute | solution.py:30
  142.8 11.4 %collective-permute-start.20 = (bf16[96,2048]{1,0:T(8,128)(2,1)S(1)}, bf16[96,2048]{1,0:T(8,128)(2,1)S(1)}, u32[]{:S(2)}, u32[]{:S(2)}) collective-permute-start(bf16[96,2048]{1,0:T(8,128)(2,1)S(1)} %shard_map.101.refs_1_.h), channel_id=1, source_target_pairs={{6,0},{0,2},{2,4},{4,6},{7,1},{1,3},{3,5},{5,7},{14,8},{8,10},{10,... | collective-permute-start | bytes 1179656 | tf_op jit(solution)/shard_map/ppermute | solution.py:30
  142.9 18.5 %collective-permute-start.21 = (bf16[96,2048]{1,0:T(8,128)(2,1)S(1)}, bf16[96,2048]{1,0:T(8,128)(2,1)S(1)}, u32[]{:S(2)}, u32[]{:S(2)}) collective-permute-start(bf16[96,2048]{1,0:T(8,128)(2,1)S(1)} %shard_map.101.refs_1_.h), channel_id=1, source_target_pairs={{4,0},{6,2},{0,4},{2,6},{5,1},{7,3},{1,5},{3,7},{12,8},{14,10},{8,... | collective-permute-start | bytes 1179656 | tf_op jit(solution)/shard_map/ppermute | solution.py:30
  144.6 18.4 %collective-permute-start.22 = (bf16[96,2048]{1,0:T(8,128)(2,1)S(1)}, bf16[96,2048]{1,0:T(8,128)(2,1)S(1)}, u32[]{:S(2)}, u32[]{:S(2)}) collective-permute-start(bf16[96,2048]{1,0:T(8,128)(2,1)S(1)} %shard_map.101.refs_1_.h), channel_id=1, source_target_pairs={{2,0},{4,2},{6,4},{0,6},{3,1},{5,3},{7,5},{1,7},{10,8},{12,10},{14... | collective-permute-start | bytes 1179656 | tf_op jit(solution)/shard_map/ppermute | solution.py:30
  167.1 6.6 %collective-permute-start.34 = (bf16[128,512]{1,0:T(8,128)(2,1)S(1)}, bf16[128,512]{1,0:T(8,128)(2,1)S(1)}, u32[]{:S(2)}, u32[]{:S(2)}) collective-permute-start(bf16[128,512]{1,0:T(8,128)(2,1)S(1)} %get-tuple-element.58), channel_id=1, source_target_pairs={{0,1},{1,0},{2,3},{3,2},{4,5},{5,4},{6,7},{7,6},{8,9},{9,8},{10,11... | collective-permute-start | bytes 393224 | tf_op jit(solution)/shard_map/ppermute | solution.py:34
  168.8 4.9 %collective-permute-start.35 = (bf16[32,512]{1,0:T(8,128)(2,1)S(1)}, bf16[32,512]{1,0:T(8,128)(2,1)S(1)}, u32[]{:S(2)}, u32[]{:S(2)}) collective-permute-start(bf16[32,512]{1,0:T(8,128)(2,1)S(1)} %get-tuple-element.59), channel_id=1, source_target_pairs={{1,8},{9,16},{17,24},{25,32},{33,40},{41,48},{49,56},{57,64},{65,7... | collective-permute-start | bytes 98312 | tf_op jit(solution)/shard_map/ppermute | solution.py:287
  184.4 20.4 %collective-permute-start.36 = (bf16[96,2048]{1,0:T(8,128)(2,1)S(1)}, bf16[96,2048]{1,0:T(8,128)(2,1)S(1)}, u32[]{:S(2)}, u32[]{:S(2)}) collective-permute-start(bf16[96,2048]{1,0:T(8,128)(2,1)S(1)} %get-tuple-element.67), channel_id=1, source_target_pairs={{6,0},{0,2},{2,4},{4,6},{7,1},{1,3},{3,5},{5,7},{14,8},{8,10},{10,... | collective-permute-start | bytes 1179656 | tf_op jit(solution)/shard_map/ppermute | solution.py:30
  184.8 20.1 %collective-permute-start.37 = (bf16[96,2048]{1,0:T(8,128)(2,1)S(1)}, bf16[96,2048]{1,0:T(8,128)(2,1)S(1)}, u32[]{:S(2)}, u32[]{:S(2)}) collective-permute-start(bf16[96,2048]{1,0:T(8,128)(2,1)S(1)} %get-tuple-element.68), channel_id=1, source_target_pairs={{2,0},{4,2},{6,4},{0,6},{3,1},{5,3},{7,5},{1,7},{10,8},{12,10},{14... | collective-permute-start | bytes 1179656 | tf_op jit(solution)/shard_map/ppermute | solution.py:30
  188.6 16.3 %collective-permute-start.38 = (bf16[96,2048]{1,0:T(8,128)(2,1)S(1)}, bf16[96,2048]{1,0:T(8,128)(2,1)S(1)}, u32[]{:S(2)}, u32[]{:S(2)}) collective-permute-start(bf16[96,2048]{1,0:T(8,128)(2,1)S(1)} %shard_map.109), channel_id=1, source_target_pairs={{4,0},{6,2},{0,4},{2,6},{5,1},{7,3},{1,5},{3,7},{12,8},{14,10},{8,... | collective-permute-start | bytes 1179656 | tf_op jit(solution)/shard_map/ppermute | solution.py:30
where the time goes:
time: 208 us; the launch traced here: 206 us
  waiting for transfers between devices  105 us (50%)
  starting transfers between devices  55.7 us (27%)
  Pallas kernels  26 us (12%)
  blocking collectives  15.6 us (8%)
  local copies, waits for them, and re-layouts  3.33 us (2%)
    ppermute x31, waiting for transfers between devices, take(): return lax.ppermute(a, axis, [((i + by) % n, i) for i in range(n)])  105 us
    ppermute x31, starting transfers between devices, take(): return lax.ppermute(a, axis, [((i + by) % n, i) for i in range(n)])  39.3 us
    pallas_call x20, Pallas kernels, call(): pl.pallas_call(kernel, out_shape=[jax.ShapeDtypeStruct(s, d) for s, d in...  26 us
    all_to_all x2, blocking collectives, layer_body(): lax.all_to_all(jnp.broadcast_to(s[None], (4, 8, 128)), 'x', 0, 0, tiled=T...  15.6 us
    ppermute x6, starting transfers between devices, swap(): return lax.ppermute(a, 'c', [(0, 1), (1, 0)])  12.4 us
  transfers between devices with their start and end apart: 39, of which 17 were waited for; matrix products, arithmetic and copies ran while one was open for 0% of the time, Pallas kernels for 9%

commit v1 on v0

--- a/solution.py
+++ b/solution.py
@@ -34,7 +34,7 @@
     return lax.ppermute(a, "c", [(0, 1), (1, 0)])
 
 
-def call(kernel, outs, inputs, scratch=(), scalars=True):
+def call(kernel, outs, inputs, scratch=(), scalars=True, alias=None):
     n = len(inputs) - (1 if scalars else 0)
     vmem = pl.BlockSpec(memory_space=pltpu.VMEM)
     specs = ([pl.BlockSpec(memory_space=pltpu.SMEM)] if scalars else []) + [vmem] * n
@@ -44,6 +44,7 @@
         in_specs=specs,
         out_specs=[vmem] * len(outs),
         scratch_shapes=list(scratch),
+        input_output_aliases=alias or {},
         compiler_params=pltpu.CompilerParams(vmem_limit_bytes=12 * 1024 * 1024),
     )(*inputs)
 
@@ -91,25 +92,31 @@
         out[k * CH : (k + 1) * CH] = a[...]
 
 
-def spread(at, refs, table, dst, lanes, out_lanes):
-    for i, r, place, n in table:
-        base, step = place, PIECE
-        if isinstance(place, tuple):
-            base, step = place[1] * CH + ((at[1] + place[0]) % 4) * PIECE, CH
-
-        def piece(j, _, i=i, r=r, base=base, step=step):
-            src = pl.multiple_of(r + j * PIECE, PIECE)
-            to = pl.multiple_of(base + j * step, PIECE)
-            dst[pl.ds(to, PIECE), out_lanes] = refs[i][pl.ds(src, PIECE), lanes]
+def spread_kernel(at, *refs, table):
+    out = refs[-1]
+    for i, row, dy, first, n in table:
+        base = first * CH + ((at[1] + dy) % 4) * PIECE
+
+        def piece(j, _, i=i, row=row, base=base):
+            src = pl.multiple_of(row + j * PIECE, PIECE)
+            to = pl.multiple_of(base + j * CH, PIECE)
+            out[pl.ds(to, PIECE)] = refs[i][pl.ds(src, PIECE)]
             return 0
 
-        lax.fori_loop(0, n // PIECE, piece, 0)
-
-
-def glu_first_kernel(*refs, n, table):
-    at, own, m, f, p = refs[:5]
-    w = refs[5 : 5 + n]
-    glu, tok, scale, full = refs[5 + n :]
+        lax.fori_loop(0, n, piece, 0)
+
+
+def spread_call(at, arrays, table, into=None):
+    inputs = [at, *arrays] + ([] if into is None else [into])
+    return call(
+        functools.partial(spread_kernel, table=table),
+        [((WIDTH, BUNDLE), BF)],
+        inputs,
+        alias=None if into is None else {len(inputs) - 1: 0},
+    )[0]
+
+
+def tok_kernel(own, m, f, p, tok, scale):
     for r, a in enumerate((own, m, f, p)):
         tok[r * ROWS : (r + 1) * ROWS] = a[...]
         t = jnp.zeros((ROWS, 128), F32)
@@ -118,22 +125,21 @@
             t = t + v * v
         s = lax.rsqrt(jnp.sum(t, axis=1, keepdims=True) * (1.0 / WIDTH) + EPS)
         scale[r * ROWS : (r + 1) * ROWS] = jnp.broadcast_to(s, (ROWS, 128))
-    spread(at, w, table, full, slice(0, 2 * CH), slice(0, 2 * CH))
-    both = jnp.dot(tok[...], full[...], preferred_element_type=F32)
+
+
+def glu_of(tok, scale, w):
+    both = jnp.dot(tok[...], w[:, : 2 * CH], preferred_element_type=F32)
     s = scale[:, 0:1]
     lin, gate = both[:, :CH] * s, both[:, CH:] * s
-    glu[...] = (lin / (1.0 + jnp.exp(-gate))).astype(BF)
-
-
-def glu_second_kernel(*refs, n, table):
-    at, tok, scale, other = refs[:4]
-    w = refs[4 : 4 + n]
-    glu, tails, last, full = refs[4 + n :]
-    spread(at, w, table, full, slice(0, 2 * CH), slice(0, 2 * CH))
-    both = jnp.dot(tok[...], full[...], preferred_element_type=F32)
-    s = scale[:, 0:1]
-    lin, gate = both[:, :CH] * s, both[:, CH:] * s
-    glu[...] = (lin / (1.0 + jnp.exp(-gate))).astype(BF)
+    return (lin / (1.0 + jnp.exp(-gate))).astype(BF)
+
+
+def glu_first_kernel(tok, scale, w, glu):
+    glu[...] = glu_of(tok, scale, w)
+
+
+def glu_second_kernel(at, tok, scale, other, w, glu, tails, last):
+    glu[...] = glu_of(tok, scale, w)
     for r in range(4):
         here = slice((r + 1) * ROWS - KEEP, (r + 1) * ROWS)
         tails[r * KEEP : (r + 1) * KEEP, :CH] = other[here]
@@ -142,20 +148,15 @@
 
 
 def glu_calls(at, tokens, own, other):
-    (a, ta), (b, tb) = own, other
     size = (4 * ROWS, CH)
-    full = pltpu.VMEM((WIDTH, 2 * CH), BF)
-    glu_a, tok, scale = call(
-        functools.partial(glu_first_kernel, n=len(a), table=ta),
-        [(size, BF), ((4 * ROWS, WIDTH), BF), ((4 * ROWS, 128), F32)],
-        [at, *tokens, *a],
-        [full],
-    )
+    tok, scale = call(
+        tok_kernel, [((4 * ROWS, WIDTH), BF), ((4 * ROWS, 128), F32)], list(tokens), scalars=False
+    )
+    (glu_a,) = call(glu_first_kernel, [(size, BF)], [tok, scale, own], scalars=False)
     glu_b, tails, last = call(
-        functools.partial(glu_second_kernel, n=len(b), table=tb),
+        glu_second_kernel,
         [(size, BF), ((4 * KEEP, 2 * CH), BF), ((KEEP, 2 * CH), BF)],
-        [at, tok, scale, glu_a, *b],
-        [full],
+        [at, tok, scale, glu_a, other],
     )
     return glu_a, glu_b, tails, last
 
@@ -171,11 +172,8 @@
     return acc
 
 
-def conv_rest_kernel(*refs, n, m, tables, layer):
-    at, glu_a, glu_b = refs[:3]
-    par_a, par_b = refs[3].at[layer], refs[4].at[layer]
-    wa, wb = refs[5 : 5 + n], refs[5 + n : 5 + n + m]
-    mixed, t1, t2, wo, win = refs[5 + n + m :]
+def conv_rest_kernel(glu_a, glu_b, par_a, par_b, mixed, t1, t2, win, *, layer):
+    par_a, par_b = par_a.at[layer], par_b.at[layer]
 
     def block(r, _):
         here = pl.multiple_of(r * ROWS, KEEP)
@@ -194,8 +192,6 @@
         return 0
 
     lax.fori_loop(0, 4, block, 0)
-    spread(at, wa, tables[0], wo, slice(2 * CH, 3 * CH), slice(0, CH))
-    spread(at, wb, tables[1], wo, slice(2 * CH, 3 * CH), slice(CH, 2 * CH))
 
 
 def conv_edge_kernel(at, glu_a, glu_b, other, before, par_a, par_b, t1, t2, mixed, stats, win, l1, l2, *, layer):
@@ -233,8 +229,8 @@
 
 
 def out_kernel(*refs, blocks, layer):
-    at, low, high, stats, par_a, par_b, wo = refs[:7]
-    outs, act = refs[7:-1], refs[-1]
+    at, low, high, stats, par_a, par_b, wa, wb = refs[:8]
+    outs, act = refs[8:-1], refs[-1]
     par_a, par_b = par_a.at[layer], par_b.at[layer]
     x = at[2]
     own, m, f, p = (stats[pl.ds(pl.multiple_of(((x + d) % 4) * 8, 8), 8)] for d in (0, 3, 2, 1))
@@ -256,7 +252,9 @@
                 v = v * par[TAPS + 1 : TAPS + 2] + par[TAPS + 2 : TAPS + 3]
                 to = n * ROWS + first
                 act[to : to + size, s * CH : (s + 1) * CH] = (v / (1.0 + jnp.exp(-v))).astype(BF)
-    d = lax.dot_general(act[...], wo[...], (((1,), (1,)), ((), ())), preferred_element_type=F32)
+    dims = (((1,), (1,)), ((), ()))
+    d = lax.dot_general(act[:, :CH], wa[:, 2 * CH :], dims, preferred_element_type=F32)
+    d = d + lax.dot_general(act[:, CH:], wb[:, 2 * CH :], dims, preferred_element_type=F32)
     for n, out in enumerate(outs):
         out[...] = d[n * ROWS : (n + 1) * ROWS].astype(out.dtype)
 
@@ -286,12 +284,12 @@
     there = swap(tails)
     before = lax.ppermute(last, ("z", "y", "c"), before_pairs)
     par_a, par_b = par
-    (a, ta), (b, tb) = own, other
-    high, t1, t2, wo = call(
-        functools.partial(conv_rest_kernel, n=len(a), m=len(b), tables=(ta, tb), layer=layer),
-        [((4 * REST, 2 * CH), F32)] + [((4 * REST, 128), F32)] * 2 + [((WIDTH, 2 * CH), BF)],
-        [at, glu_a, glu_b, par_a, par_b, *a, *b],
+    high, t1, t2 = call(
+        functools.partial(conv_rest_kernel, layer=layer),
+        [((4 * REST, 2 * CH), F32)] + [((4 * REST, 128), F32)] * 2,
+        [glu_a, glu_b, par_a, par_b],
         [pltpu.VMEM((ROWS, 128), F32)],
+        scalars=False,
     )
     low, s = call(
         functools.partial(conv_edge_kernel, layer=layer),
@@ -300,7 +298,7 @@
         [pltpu.VMEM((2 * KEEP, 128), F32)] + [pltpu.VMEM((4 * KEEP, 128), F32)] * 2,
     )
     stats = lax.all_to_all(jnp.broadcast_to(s[None], (4, 8, 128)), "x", 0, 0, tiled=True)
-    inputs = (at, low, high, stats.reshape(32, 128), par_a, par_b, wo)
+    inputs = (at, low, high, stats.reshape(32, 128), par_a, par_b, own, other)
     (o2,) = out_call(layer, (2,), (BF,), *inputs)
     from_f = take(o2, "x", 2)
     o3, o1, o0 = out_call(layer, (3, 1, 0), (BF, BF, F32), *inputs)
@@ -344,16 +342,10 @@
     fu, fd = take(up[:cut], "y", 1), take(down[cut:], "y", -1)
     s2 = swap(jnp.concatenate([line, up, down], axis=0))
     s3 = swap(jnp.concatenate([fu, fd], axis=0))
-    own0 = (
-        [line, up, down, fu, fd],
-        [(0, 0, (0, 0), size), (1, 0, (1, 0), size), (2, 0, (3, 0), size)]
-        + [(3, 0, (2, 0), cut), (4, 0, (2, 4), cut)],
-    )
-    other0 = (
-        [s2, s3],
-        [(0, n * size, (dy, 0), size) for n, dy in enumerate((0, 1, 3))]
-        + [(1, 0, (2, 0), size)],
-    )
+    own0 = spread_call(at, [line, up, down], ((0, 0, 0, 0, 8), (1, 0, 1, 0, 8), (2, 0, 3, 0, 8)))
+    own0 = spread_call(at, [fu, fd], ((0, 0, 2, 0, 4), (1, 0, 2, 4, 4)), own0)
+    table = ((0, 0, 0, 0, 8), (0, size, 1, 0, 8), (0, 2 * size, 3, 0, 8), (1, 0, 2, 0, 8))
+    other0 = spread_call(at, [s2, s3], table)
 
     g = [b1, take(b1, "y", 1), take(b1, "y", 2), take(b1, "y", 3)]
     (near,) = call(near_kernel, [((CH, BUNDLE), BF)], [at, *g])
@@ -367,10 +359,8 @@
     size = lax.axis_size("z") * lax.axis_size("y")
     pairs = [(2 * i + 1, 2 * (i + 1)) for i in range(size - 1)]
     state, ready = layer_body(0, at, state, gather_tokens(state), own0, other0, par, pairs)
-    (both,) = call(cat_kernel, [((WIDTH, BUNDLE), BF)], [*chunks, ready], scalars=False)
-    ysw = swap(both)
-    own1 = (chunks, [(k, 0, k * CH, CH) for k in range(8)])
-    other1 = ([ysw], [(0, 0, 0, WIDTH)])
+    (own1,) = call(cat_kernel, [((WIDTH, BUNDLE), BF)], [*chunks, ready], scalars=False)
+    other1 = swap(own1)
     state, _ = layer_body(1, at, state, gather_tokens(state), own1, other1, par, pairs)
     return state
 

time: 208 us -> 207 us (level)
    pallas_call x20 -> x25, Pallas kernels: 26 us -> 24.2 us  [call(): pl.pallas_call(kernel, out_shape=[jax.ShapeDtypeStruct(s, d) for s, d in...]
  transfers between devices with their start and end apart: 39 -> 39, of which waited for: 17 -> 17; matrix products, arithmetic and copies ran while one was open for 0% -> 0% of each run, Pallas kernels for 9% -> 8%
where the time goes in v1:
time: 207 us; the launch traced here: 204 us
  waiting for transfers between devices  104 us (50%)
  starting transfers between devices  56.8 us (27%)
  Pallas kernels  24.2 us (12%)
  blocking collectives  15.6 us (8%)
  local copies, waits for them, and re-layouts  3.33 us (2%)
    ppermute x31, waiting for transfers between devices, take(): return lax.ppermute(a, axis, [((i + by) % n, i) for i in range(n)])  104 us
    ppermute x31, starting transfers between devices, take(): return lax.ppermute(a, axis, [((i + by) % n, i) for i in range(n)])  39.3 us
    pallas_call x25, Pallas kernels, call(): pl.pallas_call(kernel, out_shape=[jax.ShapeDtypeStruct(s, d) for s, d in...  24.2 us
    all_to_all x2, blocking collectives, layer_body(): lax.all_to_all(jnp.broadcast_to(s[None], (4, 8, 128)), 'x', 0, 0, tiled=T...  15.6 us
    ppermute x6, starting transfers between devices, swap(): return lax.ppermute(a, 'c', [(0, 1), (1, 0)])  12.4 us
    ppermute x2, starting transfers between devices, layer_body(): before = lax.ppermute(last, ('z', 'y', 'c'), before_pairs)  5.13 us
  transfers between devices with their start and end apart: 39, of which 17 were waited for; matrix products, arithmetic and copies ran while one was open for 0% of the time, Pallas kernels for 8%

profile of v1, /device:TPU:1, one launch (start us, length us, event | category | flops | bytes accessed | tf_op | source)
XLA Modules:
  0.0 204.5 jit_solution(7121639235537238585)
XLA Ops:
  4.1 6.5 %collective-permute-start.3 = (bf16[64,768]{1,0:T(8,128)(2,1)S(1)}, bf16[64,768]{1,0:T(8,128)(2,1)S(1)}, u32[]{:S(2)}, u32[]{:S(2)}) collective-permute-start(bf16[64,768]{1,0:T(8,128)(2,1)S(1)} %get-tuple-element.35.own), channel_id=1, source_target_pairs={{32,0},{64,32},{96,64},{128,96},{160,128},{192,160},{224,192},{0,2... | collective-permute-start | bytes 294920 | tf_op jit(solution)/shard_map/ppermute | solution.py:30
  10.5 1.6 collective-permute-done.3.za
  12.2 3.0 %collective-permute-done.4.zb = bf16[64,768]{1,0:T(8,128)(2,1)S(1)} collective-permute-done((bf16[64,768]{1,0:T(8,128)(2,1)S(1)}, bf16[64,768]{1,0:T(8,128)(2,1)S(1)}, u32[]{:S(2)}, u32[]{:S(2)}) %collective-permute-start.4) | collective-permute-done | bytes 98336 | tf_op jit(solution)/shard_map/ppermute | solution.py:30
  15.6 2.1 %collective-permute-start.7 = (bf16[128,768]{1,0:T(8,128)(2,1)S(1)}, bf16[128,768]{1,0:T(8,128)(2,1)S(1)}, u32[]{:S(2)}, u32[]{:S(2)}) collective-permute-start(bf16[128,768]{1,0:T(8,128)(2,1)S(1)} %get-tuple-element.61), channel_id=1, source_target_pairs={{192,0},{224,32},{0,64},{32,96},{64,128},{96,160},{128,192},{160,2... | collective-permute-start | bytes 589832 | tf_op jit(solution)/shard_map/ppermute | solution.py:30
  17.7 1.4 collective-permute-start.6
  19.1 10.2 %collective-permute-done.6.z4 = bf16[64,768]{1,0:T(8,128)(2,1)S(1)} collective-permute-done((bf16[64,768]{1,0:T(8,128)(2,1)S(1)}, bf16[64,768]{1,0:T(8,128)(2,1)S(1)}, u32[]{:S(2)}, u32[]{:S(2)}) %collective-permute-start.6) | collective-permute-done | bytes 98336 | tf_op jit(solution)/shard_map/ppermute | solution.py:30
  30.2 2.8 %collective-permute-start.8 = (bf16[512,768]{1,0:T(8,128)(2,1)S(1)}, bf16[512,768]{1,0:T(8,128)(2,1)S(1)}, u32[]{:S(2)}, u32[]{:S(2)}) collective-permute-start(bf16[512,768]{1,0:T(8,128)(2,1)S(1)} %shard_map.94.refs_0_), channel_id=1, source_target_pairs={{8,0},{16,8},{24,16},{0,24},{9,1},{17,9},{25,17},{1,25},{10,2},{18... | collective-permute-start | bytes 2359304 | tf_op jit(solution)/shard_map/ppermute | solution.py:30
  33.0 15.2 %collective-permute-done.8.refs_1_ = bf16[512,768]{1,0:T(8,128)(2,1)S(1)} collective-permute-done((bf16[512,768]{1,0:T(8,128)(2,1)S(1)}, bf16[512,768]{1,0:T(8,128)(2,1)S(1)}, u32[]{:S(2)}, u32[]{:S(2)}) %collective-permute-start.8) | collective-permute-done | bytes 786464 | tf_op jit(solution)/shard_map/ppermute | solution.py:30
  48.1 3.1 %collective-permute-done.10.refs_2_ = bf16[512,768]{1,0:T(8,128)(2,1)S(1)} collective-permute-done((bf16[512,768]{1,0:T(8,128)(2,1)S(1)}, bf16[512,768]{1,0:T(8,128)(2,1)S(1)}, u32[]{:S(2)}, u32[]{:S(2)}) %collective-permute-start.10) | collective-permute-done | bytes 786464 | tf_op jit(solution)/shard_map/ppermute | solution.py:30
  51.4 3.0 %collective-permute-start.12 = (bf16[1536,768]{1,0:T(8,128)(2,1)S(1)}, bf16[1536,768]{1,0:T(8,128)(2,1)S(1)}, u32[]{:S(2)}, u32[]{:S(2)}) collective-permute-start(bf16[1536,768]{1,0:T(8,128)(2,1)S(1)} %pad_maximum_fusion), channel_id=1, source_target_pairs={{0,1},{1,0},{2,3},{3,2},{4,5},{5,4},{6,7},{7,6},{8,9},{9,8},{10,11... | collective-permute-start | bytes 7077896 | tf_op jit(solution)/shard_map/ppermute | solution.py:34
  55.9 2.8 %collective-permute-done.23.a1 = bf16[64,768]{1,0:T(8,128)(2,1)S(1)} collective-permute-done((bf16[64,768]{1,0:T(8,128)(2,1)S(1)}, bf16[64,768]{1,0:T(8,128)(2,1)S(1)}, u32[]{:S(2)}, u32[]{:S(2)}) %collective-permute-start.23) | collective-permute-done | bytes 98336 | tf_op jit(solution)/shard_map/ppermute | solution.py:30
  58.6 1.2 collective-permute-done.24.a2
  59.9 2.9 %collective-permute-done.25.a3 = bf16[64,768]{1,0:T(8,128)(2,1)S(1)} collective-permute-done((bf16[64,768]{1,0:T(8,128)(2,1)S(1)}, bf16[64,768]{1,0:T(8,128)(2,1)S(1)}, u32[]{:S(2)}, u32[]{:S(2)}) %collective-permute-start.25) | collective-permute-done | bytes 98336 | tf_op jit(solution)/shard_map/ppermute | solution.py:30
  65.7 1.3 collective-permute-start
  67.0 6.6 %collective-permute-done.26.refs_1_ = bf16[256,768]{1,0:T(8,128)(2,1)S(1)} collective-permute-done((bf16[256,768]{1,0:T(8,128)(2,1)S(1)}, bf16[256,768]{1,0:T(8,128)(2,1)S(1)}, u32[]{:S(2)}, u32[]{:S(2)}) %collective-permute-start.26) | collective-permute-done | bytes 393248 | tf_op jit(solution)/shard_map/ppermute | solution.py:30
  73.6 1.2 collective-permute-start.30
  74.8 1.6 collective-permute-start.27
  76.4 2.7 %collective-permute-start.1 = (bf16[96,2048]{1,0:T(8,128)(2,1)S(1)}, bf16[96,2048]{1,0:T(8,128)(2,1)S(1)}, u32[]{:S(2)}, u32[]{:S(2)}) collective-permute-start(bf16[96,2048]{1,0:T(8,128)(2,1)S(1)} %shard_map.91.own.h), channel_id=1, source_target_pairs={{4,0},{6,2},{0,4},{2,6},{5,1},{7,3},{1,5},{3,7},{12,8},{14,10},{8,... | collective-permute-start | bytes 1179656 | tf_op jit(solution)/shard_map/ppermute | solution.py:30
  79.3 2.3 %collective-permute-start.13 = (bf16[512,768]{1,0:T(8,128)(2,1)S(1)}, bf16[512,768]{1,0:T(8,128)(2,1)S(1)}, u32[]{:S(2)}, u32[]{:S(2)}) collective-permute-start(bf16[512,768]{1,0:T(8,128)(2,1)S(1)} %pad_maximum_fusion.1), channel_id=1, source_target_pairs={{0,1},{1,0},{2,3},{3,2},{4,5},{5,4},{6,7},{7,6},{8,9},{9,8},{10,11... | collective-permute-start | bytes 2359304 | tf_op jit(solution)/shard_map/ppermute | solution.py:34
  81.5 2.6 %collective-permute-done.30.refs_7_ = bf16[256,768]{1,0:T(8,128)(2,1)S(1)} collective-permute-done((bf16[256,768]{1,0:T(8,128)(2,1)S(1)}, bf16[256,768]{1,0:T(8,128)(2,1)S(1)}, u32[]{:S(2)}, u32[]{:S(2)}) %collective-permute-start.30) | collective-permute-done | bytes 393248 | tf_op jit(solution)/shard_map/ppermute | solution.py:30
  84.5 2.4 %collective-permute-start.28 = (bf16[256,768]{1,0:T(8,128)(2,1)S(1)}, bf16[256,768]{1,0:T(8,128)(2,1)S(1)}, u32[]{:S(2)}, u32[]{:S(2)}) collective-permute-start(bf16[256,768]{1,0:T(8,128)(2,1)S(1)} %collective-permute-done.27.refs_2_), channel_id=1, source_target_pairs={{32,0},{64,32},{96,64},{128,96},{160,128},{192,160},{224,192},{0,2... | collective-permute-start | bytes 1179656 | tf_op jit(solution)/shard_map/ppermute | solution.py:30
  86.8 2.5 %collective-permute-start.2 = (bf16[96,2048]{1,0:T(8,128)(2,1)S(1)}, bf16[96,2048]{1,0:T(8,128)(2,1)S(1)}, u32[]{:S(2)}, u32[]{:S(2)}) collective-permute-start(bf16[96,2048]{1,0:T(8,128)(2,1)S(1)} %shard_map.91.own.h), channel_id=1, source_target_pairs={{2,0},{4,2},{6,4},{0,6},{3,1},{5,3},{7,5},{1,7},{10,8},{12,10},{14... | collective-permute-start | bytes 1179656 | tf_op jit(solution)/shard_map/ppermute | solution.py:30
  89.3 4.5 %collective-permute-done.31.refs_6_ = bf16[256,768]{1,0:T(8,128)(2,1)S(1)} collective-permute-done((bf16[256,768]{1,0:T(8,128)(2,1)S(1)}, bf16[256,768]{1,0:T(8,128)(2,1)S(1)}, u32[]{:S(2)}, u32[]{:S(2)}) %collective-permute-start.31) | collective-permute-done | bytes 393248 | tf_op jit(solution)/shard_map/ppermute | solution.py:30
  93.9 2.7 %collective-permute-start.29 = (bf16[256,768]{1,0:T(8,128)(2,1)S(1)}, bf16[256,768]{1,0:T(8,128)(2,1)S(1)}, u32[]{:S(2)}, u32[]{:S(2)}) collective-permute-start(bf16[256,768]{1,0:T(8,128)(2,1)S(1)} %collective-permute-done.28.refs_3_), channel_id=1, source_target_pairs={{32,0},{64,32},{96,64},{128,96},{160,128},{192,160},{224,192},{0,2... | collective-permute-start | bytes 1179656 | tf_op jit(solution)/shard_map/ppermute | solution.py:30
  100.4 1.5 shard_map.99
  101.9 3.7 %collective-permute-start.14 = (bf16[128,512]{1,0:T(8,128)(2,1)S(1)}, bf16[128,512]{1,0:T(8,128)(2,1)S(1)}, u32[]{:S(2)}, u32[]{:S(2)}) collective-permute-start(bf16[128,512]{1,0:T(8,128)(2,1)S(1)} %get-tuple-element.37), channel_id=1, source_target_pairs={{0,1},{1,0},{2,3},{3,2},{4,5},{5,4},{6,7},{7,6},{8,9},{9,8},{10,11... | collective-permute-start | bytes 393224 | tf_op jit(solution)/shard_map/ppermute | solution.py:34
  105.8 1.3 collective-permute-start.15
  107.1 1.3 shard_map.101
  108.4 1.4 shard_map.102
  109.8 8.0 %all_to_all.10 = f32[4,8,128]{2,1,0:T(8,128)S(1)} all-to-all(f32[4,8,128]{2,1,0:T(8,128)S(1)} %broadcast_in_dim.4), channel_id=1, replica_groups=mesh['z'=8,'y'=4,'x'=4,'c'=2] {'x'}, dimensions={0} | all-to-all | bytes 32768 | tf_op jit(solution)/shard_map/all_to_all | solution.py:300
  117.9 1.6 shard_map.103
  119.7 1.6 collective-permute-start.33
  122.8 1.4 shard_map.104
  125.2 17.0 %collective-permute-done.17.m = bf16[96,2048]{1,0:T(8,128)(2,1)S(1)} collective-permute-done((bf16[96,2048]{1,0:T(8,128)(2,1)S(1)}, bf16[96,2048]{1,0:T(8,128)(2,1)S(1)}, u32[]{:S(2)}, u32[]{:S(2)}) %collective-permute-start.17) | collective-permute-done | bytes 393248 | tf_op jit(solution)/shard_map/ppermute | solution.py:30
  143.0 1.7 collective-permute-start.21
  145.9 8.4 %collective-permute-done.20.m = bf16[96,2048]{1,0:T(8,128)(2,1)S(1)} collective-permute-done((bf16[96,2048]{1,0:T(8,128)(2,1)S(1)}, bf16[96,2048]{1,0:T(8,128)(2,1)S(1)}, u32[]{:S(2)}, u32[]{:S(2)}) %collective-permute-start.20) | collective-permute-done | bytes 393248 | tf_op jit(solution)/shard_map/ppermute | solution.py:30
  154.3 7.2 %collective-permute-done.21.f = bf16[96,2048]{1,0:T(8,128)(2,1)S(1)} collective-permute-done((bf16[96,2048]{1,0:T(8,128)(2,1)S(1)}, bf16[96,2048]{1,0:T(8,128)(2,1)S(1)}, u32[]{:S(2)}, u32[]{:S(2)}) %collective-permute-start.21) | collective-permute-done | bytes 393248 | tf_op jit(solution)/shard_map/ppermute | solution.py:30
  161.5 1.7 collective-permute-done.22.p
  164.6 1.6 shard_map.110
  166.2 1.7 collective-permute-start.34
  167.9 3.9 %collective-permute-start.35 = (bf16[32,512]{1,0:T(8,128)(2,1)S(1)}, bf16[32,512]{1,0:T(8,128)(2,1)S(1)}, u32[]{:S(2)}, u32[]{:S(2)}) collective-permute-start(bf16[32,512]{1,0:T(8,128)(2,1)S(1)} %get-tuple-element.52), channel_id=1, source_target_pairs={{1,8},{9,16},{17,24},{25,32},{33,40},{41,48},{49,56},{57,64},{65,7... | collective-permute-start | bytes 98312 | tf_op jit(solution)/shard_map/ppermute | solution.py:285
  173.0 1.4 shard_map.112
  174.5 7.6 %all_to_all.11 = f32[4,8,128]{2,1,0:T(8,128)S(1)} all-to-all(f32[4,8,128]{2,1,0:T(8,128)S(1)} %broadcast_in_dim.5), channel_id=1, replica_groups=mesh['z'=8,'y'=4,'x'=4,'c'=2] {'x'}, dimensions={0} | all-to-all | bytes 32768 | tf_op jit(solution)/shard_map/all_to_all | solution.py:300
  182.1 1.6 shard_map.113
  184.0 2.4 %collective-permute-start.37 = (bf16[96,2048]{1,0:T(8,128)(2,1)S(1)}, bf16[96,2048]{1,0:T(8,128)(2,1)S(1)}, u32[]{:S(2)}, u32[]{:S(2)}) collective-permute-start(bf16[96,2048]{1,0:T(8,128)(2,1)S(1)} %get-tuple-element.60), channel_id=1, source_target_pairs={{2,0},{4,2},{6,4},{0,6},{3,1},{5,3},{7,5},{1,7},{10,8},{12,10},{14... | collective-permute-start | bytes 1179656 | tf_op jit(solution)/shard_map/ppermute | solution.py:30
  186.4 1.4 shard_map.114
  187.9 15.0 %collective-permute-done.36.m = bf16[96,2048]{1,0:T(8,128)(2,1)S(1)} collective-permute-done((bf16[96,2048]{1,0:T(8,128)(2,1)S(1)}, bf16[96,2048]{1,0:T(8,128)(2,1)S(1)}, u32[]{:S(2)}, u32[]{:S(2)}) %collective-permute-start.36) | collective-permute-done | bytes 393248 | tf_op jit(solution)/shard_map/ppermute | solution.py:30
  202.9 1.5 shard_map.115
  (83 shorter events, 21.9 us)
Async XLA Ops:
  0.1 0.8 copy-start.1
  0.9 0.8 copy-start.2
  1.8 0.8 copy-start.3
  2.6 0.7 copy-start.5
  4.1 8.1 %collective-permute-start.3 = (bf16[64,768]{1,0:T(8,128)(2,1)S(1)}, bf16[64,768]{1,0:T(8,128)(2,1)S(1)}, u32[]{:S(2)}, u32[]{:S(2)}) collective-permute-start(bf16[64,768]{1,0:T(8,128)(2,1)S(1)} %get-tuple-element.35.own), channel_id=1, source_target_pairs={{32,0},{64,32},{96,64},{128,96},{160,128},{192,160},{224,192},{0,2... | collective-permute-start | bytes 294920 | tf_op jit(solution)/shard_map/ppermute | solution.py:30
  10.5 4.7 %collective-permute-start.4 = (bf16[64,768]{1,0:T(8,128)(2,1)S(1)}, bf16[64,768]{1,0:T(8,128)(2,1)S(1)}, u32[]{:S(2)}, u32[]{:S(2)}) collective-permute-start(bf16[64,768]{1,0:T(8,128)(2,1)S(1)} %get-tuple-element.35.own), channel_id=1, source_target_pairs={{224,0},{0,32},{32,64},{64,96},{96,128},{128,160},{160,192},{192,2... | collective-permute-start | bytes 294920 | tf_op jit(solution)/shard_map/ppermute | solution.py:30
  15.2 14.8 %collective-permute-start.5 = (bf16[128,768]{1,0:T(8,128)(2,1)S(1)}, bf16[128,768]{1,0:T(8,128)(2,1)S(1)}, u32[]{:S(2)}, u32[]{:S(2)}) collective-permute-start(bf16[128,768]{1,0:T(8,128)(2,1)S(1)} %get-tuple-element.62), channel_id=1, source_target_pairs={{64,0},{96,32},{128,64},{160,96},{192,128},{224,160},{0,192},{32,2... | collective-permute-start | bytes 589832 | tf_op jit(solution)/shard_map/ppermute | solution.py:30
  15.6 14.5 %collective-permute-start.7 = (bf16[128,768]{1,0:T(8,128)(2,1)S(1)}, bf16[128,768]{1,0:T(8,128)(2,1)S(1)}, u32[]{:S(2)}, u32[]{:S(2)}) collective-permute-start(bf16[128,768]{1,0:T(8,128)(2,1)S(1)} %get-tuple-element.61), channel_id=1, source_target_pairs={{192,0},{224,32},{0,64},{32,96},{64,128},{96,160},{128,192},{160,2... | collective-permute-start | bytes 589832 | tf_op jit(solution)/shard_map/ppermute | solution.py:30
  17.7 11.7 %collective-permute-start.6 = (bf16[64,768]{1,0:T(8,128)(2,1)S(1)}, bf16[64,768]{1,0:T(8,128)(2,1)S(1)}, u32[]{:S(2)}, u32[]{:S(2)}) collective-permute-start(bf16[64,768]{1,0:T(8,128)(2,1)S(1)} %get-tuple-element.35.own), channel_id=1, source_target_pairs={{128,0},{160,32},{192,64},{224,96},{0,128},{32,160},{64,192},{96,2... | collective-permute-start | bytes 294920 | tf_op jit(solution)/shard_map/ppermute | solution.py:30
  30.2 18.0 %collective-permute-start.8 = (bf16[512,768]{1,0:T(8,128)(2,1)S(1)}, bf16[512,768]{1,0:T(8,128)(2,1)S(1)}, u32[]{:S(2)}, u32[]{:S(2)}) collective-permute-start(bf16[512,768]{1,0:T(8,128)(2,1)S(1)} %shard_map.94.refs_0_), channel_id=1, source_target_pairs={{8,0},{16,8},{24,16},{0,24},{9,1},{17,9},{25,17},{1,25},{10,2},{18... | collective-permute-start | bytes 2359304 | tf_op jit(solution)/shard_map/ppermute | solution.py:30
  33.0 18.3 %collective-permute-start.10 = (bf16[512,768]{1,0:T(8,128)(2,1)S(1)}, bf16[512,768]{1,0:T(8,128)(2,1)S(1)}, u32[]{:S(2)}, u32[]{:S(2)}) collective-permute-start(bf16[512,768]{1,0:T(8,128)(2,1)S(1)} %shard_map.94.refs_0_), channel_id=1, source_target_pairs={{24,0},{0,8},{8,16},{16,24},{25,1},{1,9},{9,17},{17,25},{26,2},{2,... | collective-permute-start | bytes 2359304 | tf_op jit(solution)/shard_map/ppermute | solution.py:30
  51.4 13.7 %copy-start = (bf16[96,2048]{1,0:T(8,128)(2,1)S(1)}, bf16[96,2048]{1,0:T(8,128)(2,1)}, u32[]{:S(2)}) copy-start(bf16[96,2048]{1,0:T(8,128)(2,1)} %hidden.1) | copy-start | bytes 1179652
  51.4 48.0 %collective-permute-start.12 = (bf16[1536,768]{1,0:T(8,128)(2,1)S(1)}, bf16[1536,768]{1,0:T(8,128)(2,1)S(1)}, u32[]{:S(2)}, u32[]{:S(2)}) collective-permute-start(bf16[1536,768]{1,0:T(8,128)(2,1)S(1)} %pad_maximum_fusion), channel_id=1, source_target_pairs={{0,1},{1,0},{2,3},{3,2},{4,5},{5,4},{6,7},{7,6},{8,9},{9,8},{10,11... | collective-permute-start | bytes 7077896 | tf_op jit(solution)/shard_map/ppermute | solution.py:34
  54.4 4.3 %collective-permute-start.23 = (bf16[64,768]{1,0:T(8,128)(2,1)S(1)}, bf16[64,768]{1,0:T(8,128)(2,1)S(1)}, u32[]{:S(2)}, u32[]{:S(2)}) collective-permute-start(bf16[64,768]{1,0:T(8,128)(2,1)S(1)} %get-tuple-element.49.a0), channel_id=1, source_target_pairs={{8,0},{16,8},{24,16},{0,24},{9,1},{17,9},{25,17},{1,25},{10,2},{18... | collective-permute-start | bytes 294920 | tf_op jit(solution)/shard_map/ppermute | solution.py:30
  54.4 5.5 %collective-permute-start.24 = (bf16[64,768]{1,0:T(8,128)(2,1)S(1)}, bf16[64,768]{1,0:T(8,128)(2,1)S(1)}, u32[]{:S(2)}, u32[]{:S(2)}) collective-permute-start(bf16[64,768]{1,0:T(8,128)(2,1)S(1)} %get-tuple-element.49.a0), channel_id=1, source_target_pairs={{16,0},{24,8},{0,16},{8,24},{17,1},{25,9},{1,17},{9,25},{18,2},{26... | collective-permute-start | bytes 294920 | tf_op jit(solution)/shard_map/ppermute | solution.py:30
  55.0 7.8 %collective-permute-start.25 = (bf16[64,768]{1,0:T(8,128)(2,1)S(1)}, bf16[64,768]{1,0:T(8,128)(2,1)S(1)}, u32[]{:S(2)}, u32[]{:S(2)}) collective-permute-start(bf16[64,768]{1,0:T(8,128)(2,1)S(1)} %get-tuple-element.49.a0), channel_id=1, source_target_pairs={{24,0},{0,8},{8,16},{16,24},{25,1},{1,9},{9,17},{17,25},{26,2},{2,... | collective-permute-start | bytes 294920 | tf_op jit(solution)/shard_map/ppermute | solution.py:30
  63.3 10.3 %collective-permute-start.26 = (bf16[256,768]{1,0:T(8,128)(2,1)S(1)}, bf16[256,768]{1,0:T(8,128)(2,1)S(1)}, u32[]{:S(2)}, u32[]{:S(2)}) collective-permute-start(bf16[256,768]{1,0:T(8,128)(2,1)S(1)} %shard_map.107.refs_0_), channel_id=1, source_target_pairs={{32,0},{64,32},{96,64},{128,96},{160,128},{192,160},{224,192},{0,2... | collective-permute-start | bytes 1179656 | tf_op jit(solution)/shard_map/ppermute | solution.py:30
  63.4 11.4 %collective-permute-start.9 = (bf16[256,768]{1,0:T(8,128)(2,1)S(1)}, bf16[256,768]{1,0:T(8,128)(2,1)S(1)}, u32[]{:S(2)}, u32[]{:S(2)}) collective-permute-start(bf16[256,768]{1,0:T(8,128)(2,1)S(1)} %slice.8), channel_id=1, source_target_pairs={{8,0},{16,8},{24,16},{0,24},{9,1},{17,9},{25,17},{1,25},{10,2},{18... | collective-permute-start | bytes 1179656 | tf_op jit(solution)/shard_map/ppermute | solution.py:30
  64.0 12.5 %collective-permute-start.11 = (bf16[256,768]{1,0:T(8,128)(2,1)S(1)}, bf16[256,768]{1,0:T(8,128)(2,1)S(1)}, u32[]{:S(2)}, u32[]{:S(2)}) collective-permute-start(bf16[256,768]{1,0:T(8,128)(2,1)S(1)} %slice.9), channel_id=1, source_target_pairs={{24,0},{0,8},{8,16},{16,24},{25,1},{1,9},{9,17},{17,25},{26,2},{2,... | collective-permute-start | bytes 1179656 | tf_op jit(solution)/shard_map/ppermute | solution.py:30
  65.7 13.5 %collective-permute-start = (bf16[96,2048]{1,0:T(8,128)(2,1)S(1)}, bf16[96,2048]{1,0:T(8,128)(2,1)S(1)}, u32[]{:S(2)}, u32[]{:S(2)}) collective-permute-start(bf16[96,2048]{1,0:T(8,128)(2,1)S(1)} %shard_map.91.own.h), channel_id=1, source_target_pairs={{6,0},{0,2},{2,4},{4,6},{7,1},{1,3},{3,5},{5,7},{14,8},{8,10},{10,... | collective-permute-start | bytes 1179656 | tf_op jit(solution)/shard_map/ppermute | solution.py:30
  73.6 10.6 %collective-permute-start.30 = (bf16[256,768]{1,0:T(8,128)(2,1)S(1)}, bf16[256,768]{1,0:T(8,128)(2,1)S(1)}, u32[]{:S(2)}, u32[]{:S(2)}) collective-permute-start(bf16[256,768]{1,0:T(8,128)(2,1)S(1)} %shard_map.107.refs_0_), channel_id=1, source_target_pairs={{224,0},{0,32},{32,64},{64,96},{96,128},{128,160},{160,192},{192,2... | collective-permute-start | bytes 1179656 | tf_op jit(solution)/shard_map/ppermute | solution.py:30
  74.8 9.6 %collective-permute-start.27 = (bf16[256,768]{1,0:T(8,128)(2,1)S(1)}, bf16[256,768]{1,0:T(8,128)(2,1)S(1)}, u32[]{:S(2)}, u32[]{:S(2)}) collective-permute-start(bf16[256,768]{1,0:T(8,128)(2,1)S(1)} %collective-permute-done.26.refs_1_), channel_id=1, source_target_pairs={{32,0},{64,32},{96,64},{128,96},{160,128},{192,160},{224,192},{0,2... | collective-permute-start | bytes 1179656 | tf_op jit(solution)/shard_map/ppermute | solution.py:30
  76.4 10.4 %collective-permute-start.1 = (bf16[96,2048]{1,0:T(8,128)(2,1)S(1)}, bf16[96,2048]{1,0:T(8,128)(2,1)S(1)}, u32[]{:S(2)}, u32[]{:S(2)}) collective-permute-start(bf16[96,2048]{1,0:T(8,128)(2,1)S(1)} %shard_map.91.own.h), channel_id=1, source_target_pairs={{4,0},{6,2},{0,4},{2,6},{5,1},{7,3},{1,5},{3,7},{12,8},{14,10},{8,... | collective-permute-start | bytes 1179656 | tf_op jit(solution)/shard_map/ppermute | solution.py:30
  79.3 20.2 %collective-permute-start.13 = (bf16[512,768]{1,0:T(8,128)(2,1)S(1)}, bf16[512,768]{1,0:T(8,128)(2,1)S(1)}, u32[]{:S(2)}, u32[]{:S(2)}) collective-permute-start(bf16[512,768]{1,0:T(8,128)(2,1)S(1)} %pad_maximum_fusion.1), channel_id=1, source_target_pairs={{0,1},{1,0},{2,3},{3,2},{4,5},{5,4},{6,7},{7,6},{8,9},{9,8},{10,11... | collective-permute-start | bytes 2359304 | tf_op jit(solution)/shard_map/ppermute | solution.py:34
  84.1 9.7 %collective-permute-start.31 = (bf16[256,768]{1,0:T(8,128)(2,1)S(1)}, bf16[256,768]{1,0:T(8,128)(2,1)S(1)}, u32[]{:S(2)}, u32[]{:S(2)}) collective-permute-start(bf16[256,768]{1,0:T(8,128)(2,1)S(1)} %collective-permute-done.30.refs_7_), channel_id=1, source_target_pairs={{224,0},{0,32},{32,64},{64,96},{96,128},{128,160},{160,192},{192,2... | collective-permute-start | bytes 1179656 | tf_op jit(solution)/shard_map/ppermute | solution.py:30
  84.5 9.4 %collective-permute-start.28 = (bf16[256,768]{1,0:T(8,128)(2,1)S(1)}, bf16[256,768]{1,0:T(8,128)(2,1)S(1)}, u32[]{:S(2)}, u32[]{:S(2)}) collective-permute-start(bf16[256,768]{1,0:T(8,128)(2,1)S(1)} %collective-permute-done.27.refs_2_), channel_id=1, source_target_pairs={{32,0},{64,32},{96,64},{128,96},{160,128},{192,160},{224,192},{0,2... | collective-permute-start | bytes 1179656 | tf_op jit(solution)/shard_map/ppermute | solution.py:30
  86.8 9.7 %collective-permute-start.2 = (bf16[96,2048]{1,0:T(8,128)(2,1)S(1)}, bf16[96,2048]{1,0:T(8,128)(2,1)S(1)}, u32[]{:S(2)}, u32[]{:S(2)}) collective-permute-start(bf16[96,2048]{1,0:T(8,128)(2,1)S(1)} %shard_map.91.own.h), channel_id=1, source_target_pairs={{2,0},{4,2},{6,4},{0,6},{3,1},{5,3},{7,5},{1,7},{10,8},{12,10},{14... | collective-permute-start | bytes 1179656 | tf_op jit(solution)/shard_map/ppermute | solution.py:30
  93.8 25.6 %collective-permute-start.32 = (bf16[256,768]{1,0:T(8,128)(2,1)S(1)}, bf16[256,768]{1,0:T(8,128)(2,1)S(1)}, u32[]{:S(2)}, u32[]{:S(2)}) collective-permute-start(bf16[256,768]{1,0:T(8,128)(2,1)S(1)} %collective-permute-done.31.refs_6_), channel_id=1, source_target_pairs={{224,0},{0,32},{32,64},{64,96},{96,128},{128,160},{160,192},{192,2... | collective-permute-start | bytes 1179656 | tf_op jit(solution)/shard_map/ppermute | solution.py:30
  93.9 25.6 %collective-permute-start.29 = (bf16[256,768]{1,0:T(8,128)(2,1)S(1)}, bf16[256,768]{1,0:T(8,128)(2,1)S(1)}, u32[]{:S(2)}, u32[]{:S(2)}) collective-permute-start(bf16[256,768]{1,0:T(8,128)(2,1)S(1)} %collective-permute-done.28.refs_3_), channel_id=1, source_target_pairs={{32,0},{64,32},{96,64},{128,96},{160,128},{192,160},{224,192},{0,2... | collective-permute-start | bytes 1179656 | tf_op jit(solution)/shard_map/ppermute | solution.py:30
  100.3 5.3 %copy-start.4 = (f32[2,31,256]{2,0,1:T(2,128)S(1)}, f32[2,31,256]{2,0,1:T(2,128)}, u32[]{:S(2)}) copy-start(f32[2,31,256]{2,0,1:T(2,128)} %param.13) | copy-start | bytes 190468
  100.3 5.3 %copy-start.6 = (f32[2,256]{1,0:T(2,128)S(1)}, f32[2,256]{1,0:T(2,128)}, u32[]{:S(2)}) copy-start(f32[2,256]{1,0:T(2,128)} %cb.1) | copy-start | bytes 6148
  100.3 5.3 %copy-start.7 = (f32[2,256]{1,0:T(2,128)S(1)}, f32[2,256]{1,0:T(2,128)}, u32[]{:S(2)}) copy-start(f32[2,256]{1,0:T(2,128)} %cg.1) | copy-start | bytes 6148
  100.4 5.3 %copy-start.8 = (f32[2,256]{1,0:T(2,128)S(1)}, f32[2,256]{1,0:T(2,128)}, u32[]{:S(2)}) copy-start(f32[2,256]{1,0:T(2,128)} %cs.1) | copy-start | bytes 6148
  101.9 6.4 %collective-permute-start.14 = (bf16[128,512]{1,0:T(8,128)(2,1)S(1)}, bf16[128,512]{1,0:T(8,128)(2,1)S(1)}, u32[]{:S(2)}, u32[]{:S(2)}) collective-permute-start(bf16[128,512]{1,0:T(8,128)(2,1)S(1)} %get-tuple-element.37), channel_id=1, source_target_pairs={{0,1},{1,0},{2,3},{3,2},{4,5},{5,4},{6,7},{7,6},{8,9},{9,8},{10,11... | collective-permute-start | bytes 393224 | tf_op jit(solution)/shard_map/ppermute | solution.py:34
  105.7 1.4 collective-permute-start.16
  105.8 2.6 %collective-permute-start.15 = (bf16[32,512]{1,0:T(8,128)(2,1)S(1)}, bf16[32,512]{1,0:T(8,128)(2,1)S(1)}, u32[]{:S(2)}, u32[]{:S(2)}) collective-permute-start(bf16[32,512]{1,0:T(8,128)(2,1)S(1)} %get-tuple-element.38), channel_id=1, source_target_pairs={{1,8},{9,16},{17,24},{25,32},{33,40},{41,48},{49,56},{57,64},{65,7... | collective-permute-start | bytes 98312 | tf_op jit(solution)/shard_map/ppermute | solution.py:285
  119.7 44.9 %collective-permute-start.33 = (bf16[2048,768]{1,0:T(8,128)(2,1)S(1)}, bf16[2048,768]{1,0:T(8,128)(2,1)S(1)}, u32[]{:S(2)}, u32[]{:S(2)}) collective-permute-start(bf16[2048,768]{1,0:T(8,128)(2,1)S(1)} %shard_map.108.w.refs_6_), channel_id=1, source_target_pairs={{0,1},{1,0},{2,3},{3,2},{4,5},{5,4},{6,7},{7,6},{8,9},{9,8},{10,11... | collective-permute-start | bytes 9437192 | tf_op jit(solution)/shard_map/ppermute | solution.py:34
  121.3 20.8 %collective-permute-start.18 = (bf16[96,2048]{1,0:T(8,128)(2,1)S(1)}, bf16[96,2048]{1,0:T(8,128)(2,1)S(1)}, u32[]{:S(2)}, u32[]{:S(2)}) collective-permute-start(bf16[96,2048]{1,0:T(8,128)(2,1)S(1)} %get-tuple-element.46.refs_8_), channel_id=1, source_target_pairs={{2,0},{4,2},{6,4},{0,6},{3,1},{5,3},{7,5},{1,7},{10,8},{12,10},{14... | collective-permute-start | bytes 1179656 | tf_op jit(solution)/shard_map/ppermute | solution.py:30
  122.2 19.9 %collective-permute-start.17 = (bf16[96,2048]{1,0:T(8,128)(2,1)S(1)}, bf16[96,2048]{1,0:T(8,128)(2,1)S(1)}, u32[]{:S(2)}, u32[]{:S(2)}) collective-permute-start(bf16[96,2048]{1,0:T(8,128)(2,1)S(1)} %get-tuple-element.45), channel_id=1, source_target_pairs={{6,0},{0,2},{2,4},{4,6},{7,1},{1,3},{3,5},{5,7},{14,8},{8,10},{10,... | collective-permute-start | bytes 1179656 | tf_op jit(solution)/shard_map/ppermute | solution.py:30
  124.2 17.9 %collective-permute-start.19 = (bf16[96,2048]{1,0:T(8,128)(2,1)S(1)}, bf16[96,2048]{1,0:T(8,128)(2,1)S(1)}, u32[]{:S(2)}, u32[]{:S(2)}) collective-permute-start(bf16[96,2048]{1,0:T(8,128)(2,1)S(1)} %shard_map.104), channel_id=1, source_target_pairs={{4,0},{6,2},{0,4},{2,6},{5,1},{7,3},{1,5},{3,7},{12,8},{14,10},{8,... | collective-permute-start | bytes 1179656 | tf_op jit(solution)/shard_map/ppermute | solution.py:30
  142.9 11.4 %collective-permute-start.20 = (bf16[96,2048]{1,0:T(8,128)(2,1)S(1)}, bf16[96,2048]{1,0:T(8,128)(2,1)S(1)}, u32[]{:S(2)}, u32[]{:S(2)}) collective-permute-start(bf16[96,2048]{1,0:T(8,128)(2,1)S(1)} %shard_map.105.own.h), channel_id=1, source_target_pairs={{6,0},{0,2},{2,4},{4,6},{7,1},{1,3},{3,5},{5,7},{14,8},{8,10},{10,... | collective-permute-start | bytes 1179656 | tf_op jit(solution)/shard_map/ppermute | solution.py:30
  143.0 18.5 %collective-permute-start.21 = (bf16[96,2048]{1,0:T(8,128)(2,1)S(1)}, bf16[96,2048]{1,0:T(8,128)(2,1)S(1)}, u32[]{:S(2)}, u32[]{:S(2)}) collective-permute-start(bf16[96,2048]{1,0:T(8,128)(2,1)S(1)} %shard_map.105.own.h), channel_id=1, source_target_pairs={{4,0},{6,2},{0,4},{2,6},{5,1},{7,3},{1,5},{3,7},{12,8},{14,10},{8,... | collective-permute-start | bytes 1179656 | tf_op jit(solution)/shard_map/ppermute | solution.py:30
  144.7 18.4 %collective-permute-start.22 = (bf16[96,2048]{1,0:T(8,128)(2,1)S(1)}, bf16[96,2048]{1,0:T(8,128)(2,1)S(1)}, u32[]{:S(2)}, u32[]{:S(2)}) collective-permute-start(bf16[96,2048]{1,0:T(8,128)(2,1)S(1)} %shard_map.105.own.h), channel_id=1, source_target_pairs={{2,0},{4,2},{6,4},{0,6},{3,1},{5,3},{7,5},{1,7},{10,8},{12,10},{14... | collective-permute-start | bytes 1179656 | tf_op jit(solution)/shard_map/ppermute | solution.py:30
  166.2 6.8 %collective-permute-start.34 = (bf16[128,512]{1,0:T(8,128)(2,1)S(1)}, bf16[128,512]{1,0:T(8,128)(2,1)S(1)}, u32[]{:S(2)}, u32[]{:S(2)}) collective-permute-start(bf16[128,512]{1,0:T(8,128)(2,1)S(1)} %get-tuple-element.51), channel_id=1, source_target_pairs={{0,1},{1,0},{2,3},{3,2},{4,5},{5,4},{6,7},{7,6},{8,9},{9,8},{10,11... | collective-permute-start | bytes 393224 | tf_op jit(solution)/shard_map/ppermute | solution.py:34
  167.9 5.1 %collective-permute-start.35 = (bf16[32,512]{1,0:T(8,128)(2,1)S(1)}, bf16[32,512]{1,0:T(8,128)(2,1)S(1)}, u32[]{:S(2)}, u32[]{:S(2)}) collective-permute-start(bf16[32,512]{1,0:T(8,128)(2,1)S(1)} %get-tuple-element.52), channel_id=1, source_target_pairs={{1,8},{9,16},{17,24},{25,32},{33,40},{41,48},{49,56},{57,64},{65,7... | collective-permute-start | bytes 98312 | tf_op jit(solution)/shard_map/ppermute | solution.py:285
  183.6 19.3 %collective-permute-start.36 = (bf16[96,2048]{1,0:T(8,128)(2,1)S(1)}, bf16[96,2048]{1,0:T(8,128)(2,1)S(1)}, u32[]{:S(2)}, u32[]{:S(2)}) collective-permute-start(bf16[96,2048]{1,0:T(8,128)(2,1)S(1)} %get-tuple-element.59), channel_id=1, source_target_pairs={{6,0},{0,2},{2,4},{4,6},{7,1},{1,3},{3,5},{5,7},{14,8},{8,10},{10,... | collective-permute-start | bytes 1179656 | tf_op jit(solution)/shard_map/ppermute | solution.py:30
  184.0 18.9 %collective-permute-start.37 = (bf16[96,2048]{1,0:T(8,128)(2,1)S(1)}, bf16[96,2048]{1,0:T(8,128)(2,1)S(1)}, u32[]{:S(2)}, u32[]{:S(2)}) collective-permute-start(bf16[96,2048]{1,0:T(8,128)(2,1)S(1)} %get-tuple-element.60), channel_id=1, source_target_pairs={{2,0},{4,2},{6,4},{0,6},{3,1},{5,3},{7,5},{1,7},{10,8},{12,10},{14... | collective-permute-start | bytes 1179656 | tf_op jit(solution)/shard_map/ppermute | solution.py:30
  187.8 15.1 %collective-permute-start.38 = (bf16[96,2048]{1,0:T(8,128)(2,1)S(1)}, bf16[96,2048]{1,0:T(8,128)(2,1)S(1)}, u32[]{:S(2)}, u32[]{:S(2)}) collective-permute-start(bf16[96,2048]{1,0:T(8,128)(2,1)S(1)} %shard_map.114), channel_id=1, source_target_pairs={{4,0},{6,2},{0,4},{2,6},{5,1},{7,3},{1,5},{3,7},{12,8},{14,10},{8,... | collective-permute-start | bytes 1179656 | tf_op jit(solution)/shard_map/ppermute | solution.py:30

commit v2 on v1

--- a/solution.py
+++ b/solution.py
@@ -34,14 +34,16 @@
     return lax.ppermute(a, "c", [(0, 1), (1, 0)])
 
 
-def call(kernel, outs, inputs, scratch=(), scalars=True, alias=None):
-    n = len(inputs) - (1 if scalars else 0)
+def call(kernel, outs, inputs, scratch=(), placed=True, alias=None):
     vmem = pl.BlockSpec(memory_space=pltpu.VMEM)
-    specs = ([pl.BlockSpec(memory_space=pltpu.SMEM)] if scalars else []) + [vmem] * n
+
+    def placed_kernel(*refs):
+        kernel(tuple(lax.axis_index(a) for a in SP_TP), *refs)
+
     return pl.pallas_call(
-        kernel,
+        placed_kernel if placed else kernel,
         out_shape=[jax.ShapeDtypeStruct(s, d) for s, d in outs],
-        in_specs=specs,
+        in_specs=[vmem] * len(inputs),
         out_specs=[vmem] * len(outs),
         scratch_shapes=list(scratch),
         input_output_aliases=alias or {},
@@ -106,8 +108,8 @@
         lax.fori_loop(0, n, piece, 0)
 
 
-def spread_call(at, arrays, table, into=None):
-    inputs = [at, *arrays] + ([] if into is None else [into])
+def spread_call(arrays, table, into=None):
+    inputs = [*arrays] + ([] if into is None else [into])
     return call(
         functools.partial(spread_kernel, table=table),
         [((WIDTH, BUNDLE), BF)],
@@ -147,16 +149,16 @@
     last[...] = tails[pl.ds(pl.multiple_of(((at[2] + 1) % 4) * KEEP, KEEP), KEEP)]
 
 
-def glu_calls(at, tokens, own, other):
+def glu_calls(tokens, own, other):
     size = (4 * ROWS, CH)
     tok, scale = call(
-        tok_kernel, [((4 * ROWS, WIDTH), BF), ((4 * ROWS, 128), F32)], list(tokens), scalars=False
-    )
-    (glu_a,) = call(glu_first_kernel, [(size, BF)], [tok, scale, own], scalars=False)
+        tok_kernel, [((4 * ROWS, WIDTH), BF), ((4 * ROWS, 128), F32)], list(tokens), placed=False
+    )
+    (glu_a,) = call(glu_first_kernel, [(size, BF)], [tok, scale, own], placed=False)
     glu_b, tails, last = call(
         glu_second_kernel,
         [(size, BF), ((4 * KEEP, 2 * CH), BF), ((KEEP, 2 * CH), BF)],
-        [at, tok, scale, glu_a, other],
+        [tok, scale, glu_a, other],
     )
     return glu_a, glu_b, tails, last
 
@@ -279,8 +281,8 @@
     )
 
 
-def layer_body(layer, at, state, tokens, own, other, par, before_pairs):
-    glu_a, glu_b, tails, last = glu_calls(at, tokens, own, other)
+def layer_body(layer, state, tokens, own, other, par, before_pairs):
+    glu_a, glu_b, tails, last = glu_calls(tokens, own, other)
     there = swap(tails)
     before = lax.ppermute(last, ("z", "y", "c"), before_pairs)
     par_a, par_b = par
@@ -289,16 +291,16 @@
         [((4 * REST, 2 * CH), F32)] + [((4 * REST, 128), F32)] * 2,
         [glu_a, glu_b, par_a, par_b],
         [pltpu.VMEM((ROWS, 128), F32)],
-        scalars=False,
+        placed=False,
     )
     low, s = call(
         functools.partial(conv_edge_kernel, layer=layer),
         [((4 * KEEP, 2 * CH), F32), ((8, 128), F32)],
-        [at, glu_a, glu_b, there, before, par_a, par_b, t1, t2],
+        [glu_a, glu_b, there, before, par_a, par_b, t1, t2],
         [pltpu.VMEM((2 * KEEP, 128), F32)] + [pltpu.VMEM((4 * KEEP, 128), F32)] * 2,
     )
     stats = lax.all_to_all(jnp.broadcast_to(s[None], (4, 8, 128)), "x", 0, 0, tiled=True)
-    inputs = (at, low, high, stats.reshape(32, 128), par_a, par_b, own, other)
+    inputs = (low, high, stats.reshape(32, 128), par_a, par_b, own, other)
     (o2,) = out_call(layer, (2,), (BF,), *inputs)
     from_f = take(o2, "x", 2)
     o3, o1, o0 = out_call(layer, (3, 1, 0), (BF, BF, F32), *inputs)
@@ -306,7 +308,7 @@
     (state,) = call(
         functools.partial(add_kernel, last=layer == 1),
         [((ROWS, WIDTH), BF)],
-        [at, state, o0, from_m, from_p, from_f],
+        [state, o0, from_m, from_p, from_f],
     )
     return state, o1
 
@@ -317,38 +319,36 @@
 
 
 def body(hidden, norm_gain, w_value, w_gate, conv_weight, conv_bias, chan_gain, chan_shift, w_out):
-    z, y, x, c = (lax.axis_index(a) for a in SP_TP)
-    at = jnp.stack([z, y, x, c]).astype(jnp.int32)
     b0, b1 = call(
         fold_kernel,
         [((PIECE, BUNDLE), BF)] * 2,
-        [at, norm_gain, w_value, w_gate, w_out.swapaxes(1, 2)],
+        [norm_gain, w_value, w_gate, w_out.swapaxes(1, 2)],
         [pltpu.VMEM((128, 128), F32)],
     )
-    (state,) = call(roll_kernel, [((ROWS, WIDTH), BF)], [at, hidden])
+    (state,) = call(roll_kernel, [((ROWS, WIDTH), BF)], [hidden])
     (small,) = call(
         par_kernel,
         [((2, 40, CH), F32)],
         [conv_weight.swapaxes(0, 1), conv_bias, chan_gain, chan_shift],
-        scalars=False,
+        placed=False,
     )
 
     za, zb, z4 = take(b0, "z", 1), take(b0, "z", -1), take(b0, "z", 4)
     z2 = take(jnp.concatenate([b0, za], axis=0), "z", 2)
     z6 = take(jnp.concatenate([b0, zb], axis=0), "z", -2)
     size, cut = 8 * PIECE, 4 * PIECE
-    (line,) = call(line_kernel, [((size, BUNDLE), BF)], [b0, za, zb, z2, z4, z6], scalars=False)
+    (line,) = call(line_kernel, [((size, BUNDLE), BF)], [b0, za, zb, z2, z4, z6], placed=False)
     up, down = take(line, "y", 1), take(line, "y", -1)
     fu, fd = take(up[:cut], "y", 1), take(down[cut:], "y", -1)
     s2 = swap(jnp.concatenate([line, up, down], axis=0))
     s3 = swap(jnp.concatenate([fu, fd], axis=0))
-    own0 = spread_call(at, [line, up, down], ((0, 0, 0, 0, 8), (1, 0, 1, 0, 8), (2, 0, 3, 0, 8)))
-    own0 = spread_call(at, [fu, fd], ((0, 0, 2, 0, 4), (1, 0, 2, 4, 4)), own0)
+    own0 = spread_call([line, up, down], ((0, 0, 0, 0, 8), (1, 0, 1, 0, 8), (2, 0, 3, 0, 8)))
+    own0 = spread_call([fu, fd], ((0, 0, 2, 0, 4), (1, 0, 2, 4, 4)), own0)
     table = ((0, 0, 0, 0, 8), (0, size, 1, 0, 8), (0, 2 * size, 3, 0, 8), (1, 0, 2, 0, 8))
-    other0 = spread_call(at, [s2, s3], table)
+    other0 = spread_call([s2, s3], table)
 
     g = [b1, take(b1, "y", 1), take(b1, "y", 2), take(b1, "y", 3)]
-    (near,) = call(near_kernel, [((CH, BUNDLE), BF)], [at, *g])
+    (near,) = call(near_kernel, [((CH, BUNDLE), BF)], [*g])
     p1, m1 = take(near, "z", 1), take(near, "z", -1)
     p2, m2 = take(p1, "z", 1), take(m1, "z", -1)
     p3, m3 = take(p2, "z", 1), take(m2, "z", -1)
@@ -358,10 +358,10 @@
     par = (small, swap(small))
     size = lax.axis_size("z") * lax.axis_size("y")
     pairs = [(2 * i + 1, 2 * (i + 1)) for i in range(size - 1)]
-    state, ready = layer_body(0, at, state, gather_tokens(state), own0, other0, par, pairs)
-    (own1,) = call(cat_kernel, [((WIDTH, BUNDLE), BF)], [*chunks, ready], scalars=False)
+    state, ready = layer_body(0, state, gather_tokens(state), own0, other0, par, pairs)
+    (own1,) = call(cat_kernel, [((WIDTH, BUNDLE), BF)], [*chunks, ready], placed=False)
     other1 = swap(own1)
-    state, _ = layer_body(1, at, state, gather_tokens(state), own1, other1, par, pairs)
+    state, _ = layer_body(1, state, gather_tokens(state), own1, other1, par, pairs)
     return state
 
 

time: 207 us -> 200 us (0.966)
  Pallas kernels: 24.2 us -> 15.4 us
    pallas_call x25, Pallas kernels: 24.2 us -> 15.4 us  [call(): pl.pallas_call(placed_kernel if placed else kernel, out_shape=[jax.ShapeD...]
  transfers between devices with their start and end apart: 39 -> 39, of which waited for: 17 -> 17; matrix products, arithmetic and copies ran while one was open for 0% -> 0% of each run, Pallas kernels for 8% -> 6%
where the time goes in v2:
time: 200 us; the launch traced here: 197 us
  waiting for transfers between devices  105 us (52%)
  starting transfers between devices  56.9 us (28%)
  blocking collectives  15.6 us (8%)
  Pallas kernels  15.4 us (8%)
  local copies, waits for them, and re-layouts  3.33 us (2%)
    ppermute x31, waiting for transfers between devices, take(): return lax.ppermute(a, axis, [((i + by) % n, i) for i in range(n)])  105 us
    ppermute x31, starting transfers between devices, take(): return lax.ppermute(a, axis, [((i + by) % n, i) for i in range(n)])  39.3 us
    all_to_all x2, blocking collectives, layer_body(): lax.all_to_all(jnp.broadcast_to(s[None], (4, 8, 128)), 'x', 0, 0, tiled=T...  15.6 us
    pallas_call x25, Pallas kernels, call(): pl.pallas_call(placed_kernel if placed else kernel, out_shape=[jax.ShapeD...  15.4 us
    ppermute x6, starting transfers between devices, swap(): return lax.ppermute(a, 'c', [(0, 1), (1, 0)])  12.4 us
    ppermute x2, starting transfers between devices, layer_body(): before = lax.ppermute(last, ('z', 'y', 'c'), before_pairs)  5.21 us
  transfers between devices with their start and end apart: 39, of which 17 were waited for; matrix products, arithmetic and copies ran while one was open for 0% of the time, Pallas kernels for 6%

profile of v2, /device:TPU:1, one launch (start us, length us, event | category | flops | bytes accessed | tf_op | source)
XLA Modules:
  0.0 197.2 jit_solution(10295215797008351368)
XLA Ops:
  3.4 6.5 %collective-permute-start.3 = (bf16[64,768]{1,0:T(8,128)(2,1)S(1)}, bf16[64,768]{1,0:T(8,128)(2,1)S(1)}, u32[]{:S(2)}, u32[]{:S(2)}) collective-permute-start(bf16[64,768]{1,0:T(8,128)(2,1)S(1)} %get-tuple-element.35.own), channel_id=1, source_target_pairs={{32,0},{64,32},{96,64},{128,96},{160,128},{192,160},{224,192},{0,2... | collective-permute-start | bytes 294920 | tf_op jit(solution)/shard_map/ppermute | solution.py:30
  9.9 1.6 collective-permute-done.3.za
  11.6 3.0 %collective-permute-done.4.zb = bf16[64,768]{1,0:T(8,128)(2,1)S(1)} collective-permute-done((bf16[64,768]{1,0:T(8,128)(2,1)S(1)}, bf16[64,768]{1,0:T(8,128)(2,1)S(1)}, u32[]{:S(2)}, u32[]{:S(2)}) %collective-permute-start.4) | collective-permute-done | bytes 98336 | tf_op jit(solution)/shard_map/ppermute | solution.py:30
  15.0 2.1 %collective-permute-start.7 = (bf16[128,768]{1,0:T(8,128)(2,1)S(1)}, bf16[128,768]{1,0:T(8,128)(2,1)S(1)}, u32[]{:S(2)}, u32[]{:S(2)}) collective-permute-start(bf16[128,768]{1,0:T(8,128)(2,1)S(1)} %get-tuple-element.61), channel_id=1, source_target_pairs={{192,0},{224,32},{0,64},{32,96},{64,128},{96,160},{128,192},{160,2... | collective-permute-start | bytes 589832 | tf_op jit(solution)/shard_map/ppermute | solution.py:30
  17.1 1.4 collective-permute-start.6
  18.5 10.2 %collective-permute-done.6.z4 = bf16[64,768]{1,0:T(8,128)(2,1)S(1)} collective-permute-done((bf16[64,768]{1,0:T(8,128)(2,1)S(1)}, bf16[64,768]{1,0:T(8,128)(2,1)S(1)}, u32[]{:S(2)}, u32[]{:S(2)}) %collective-permute-start.6) | collective-permute-done | bytes 98336 | tf_op jit(solution)/shard_map/ppermute | solution.py:30
  29.5 2.8 %collective-permute-start.8 = (bf16[512,768]{1,0:T(8,128)(2,1)S(1)}, bf16[512,768]{1,0:T(8,128)(2,1)S(1)}, u32[]{:S(2)}, u32[]{:S(2)}) collective-permute-start(bf16[512,768]{1,0:T(8,128)(2,1)S(1)} %shard_map.94.refs_0_), channel_id=1, source_target_pairs={{8,0},{16,8},{24,16},{0,24},{9,1},{17,9},{25,17},{1,25},{10,2},{18... | collective-permute-start | bytes 2359304 | tf_op jit(solution)/shard_map/ppermute | solution.py:30
  32.3 15.2 %collective-permute-done.8.refs_1_ = bf16[512,768]{1,0:T(8,128)(2,1)S(1)} collective-permute-done((bf16[512,768]{1,0:T(8,128)(2,1)S(1)}, bf16[512,768]{1,0:T(8,128)(2,1)S(1)}, u32[]{:S(2)}, u32[]{:S(2)}) %collective-permute-start.8) | collective-permute-done | bytes 786464 | tf_op jit(solution)/shard_map/ppermute | solution.py:30
  47.5 3.1 %collective-permute-done.10.refs_2_ = bf16[512,768]{1,0:T(8,128)(2,1)S(1)} collective-permute-done((bf16[512,768]{1,0:T(8,128)(2,1)S(1)}, bf16[512,768]{1,0:T(8,128)(2,1)S(1)}, u32[]{:S(2)}, u32[]{:S(2)}) %collective-permute-start.10) | collective-permute-done | bytes 786464 | tf_op jit(solution)/shard_map/ppermute | solution.py:30
  50.8 3.0 %collective-permute-start.12 = (bf16[1536,768]{1,0:T(8,128)(2,1)S(1)}, bf16[1536,768]{1,0:T(8,128)(2,1)S(1)}, u32[]{:S(2)}, u32[]{:S(2)}) collective-permute-start(bf16[1536,768]{1,0:T(8,128)(2,1)S(1)} %pad_maximum_fusion), channel_id=1, source_target_pairs={{0,1},{1,0},{2,3},{3,2},{4,5},{5,4},{6,7},{7,6},{8,9},{9,8},{10,11... | collective-permute-start | bytes 7077896 | tf_op jit(solution)/shard_map/ppermute | solution.py:34
  55.2 2.8 %collective-permute-done.23.refs_1_ = bf16[64,768]{1,0:T(8,128)(2,1)S(1)} collective-permute-done((bf16[64,768]{1,0:T(8,128)(2,1)S(1)}, bf16[64,768]{1,0:T(8,128)(2,1)S(1)}, u32[]{:S(2)}, u32[]{:S(2)}) %collective-permute-start.23) | collective-permute-done | bytes 98336 | tf_op jit(solution)/shard_map/ppermute | solution.py:30
  58.0 1.2 collective-permute-done.24.refs_2_
  59.3 2.9 %collective-permute-done.25.refs_3_ = bf16[64,768]{1,0:T(8,128)(2,1)S(1)} collective-permute-done((bf16[64,768]{1,0:T(8,128)(2,1)S(1)}, bf16[64,768]{1,0:T(8,128)(2,1)S(1)}, u32[]{:S(2)}, u32[]{:S(2)}) %collective-permute-start.25) | collective-permute-done | bytes 98336 | tf_op jit(solution)/shard_map/ppermute | solution.py:30
  62.8 1.1 collective-permute-start.11
  64.0 1.3 collective-permute-start
  65.3 7.1 %collective-permute-done.26.refs_1_ = bf16[256,768]{1,0:T(8,128)(2,1)S(1)} collective-permute-done((bf16[256,768]{1,0:T(8,128)(2,1)S(1)}, bf16[256,768]{1,0:T(8,128)(2,1)S(1)}, u32[]{:S(2)}, u32[]{:S(2)}) %collective-permute-start.26) | collective-permute-done | bytes 393248 | tf_op jit(solution)/shard_map/ppermute | solution.py:30
  72.4 1.2 collective-permute-start.30
  73.7 1.6 collective-permute-start.27
  75.3 2.7 %collective-permute-start.1 = (bf16[96,2048]{1,0:T(8,128)(2,1)S(1)}, bf16[96,2048]{1,0:T(8,128)(2,1)S(1)}, u32[]{:S(2)}, u32[]{:S(2)}) collective-permute-start(bf16[96,2048]{1,0:T(8,128)(2,1)S(1)} %shard_map.91.own.refs_0_), channel_id=1, source_target_pairs={{4,0},{6,2},{0,4},{2,6},{5,1},{7,3},{1,5},{3,7},{12,8},{14,10},{8,... | collective-permute-start | bytes 1179656 | tf_op jit(solution)/shard_map/ppermute | solution.py:30
  78.1 2.3 %collective-permute-start.13 = (bf16[512,768]{1,0:T(8,128)(2,1)S(1)}, bf16[512,768]{1,0:T(8,128)(2,1)S(1)}, u32[]{:S(2)}, u32[]{:S(2)}) collective-permute-start(bf16[512,768]{1,0:T(8,128)(2,1)S(1)} %pad_maximum_fusion.1), channel_id=1, source_target_pairs={{0,1},{1,0},{2,3},{3,2},{4,5},{5,4},{6,7},{7,6},{8,9},{9,8},{10,11... | collective-permute-start | bytes 2359304 | tf_op jit(solution)/shard_map/ppermute | solution.py:34
  80.3 2.6 %collective-permute-done.30.refs_7_ = bf16[256,768]{1,0:T(8,128)(2,1)S(1)} collective-permute-done((bf16[256,768]{1,0:T(8,128)(2,1)S(1)}, bf16[256,768]{1,0:T(8,128)(2,1)S(1)}, u32[]{:S(2)}, u32[]{:S(2)}) %collective-permute-start.30) | collective-permute-done | bytes 393248 | tf_op jit(solution)/shard_map/ppermute | solution.py:30
  83.3 2.4 %collective-permute-start.28 = (bf16[256,768]{1,0:T(8,128)(2,1)S(1)}, bf16[256,768]{1,0:T(8,128)(2,1)S(1)}, u32[]{:S(2)}, u32[]{:S(2)}) collective-permute-start(bf16[256,768]{1,0:T(8,128)(2,1)S(1)} %collective-permute-done.27.refs_2_), channel_id=1, source_target_pairs={{32,0},{64,32},{96,64},{128,96},{160,128},{192,160},{224,192},{0,2... | collective-permute-start | bytes 1179656 | tf_op jit(solution)/shard_map/ppermute | solution.py:30
  85.7 2.5 %collective-permute-start.2 = (bf16[96,2048]{1,0:T(8,128)(2,1)S(1)}, bf16[96,2048]{1,0:T(8,128)(2,1)S(1)}, u32[]{:S(2)}, u32[]{:S(2)}) collective-permute-start(bf16[96,2048]{1,0:T(8,128)(2,1)S(1)} %shard_map.91.own.refs_0_), channel_id=1, source_target_pairs={{2,0},{4,2},{6,4},{0,6},{3,1},{5,3},{7,5},{1,7},{10,8},{12,10},{14... | collective-permute-start | bytes 1179656 | tf_op jit(solution)/shard_map/ppermute | solution.py:30
  88.1 4.5 %collective-permute-done.31.refs_6_ = bf16[256,768]{1,0:T(8,128)(2,1)S(1)} collective-permute-done((bf16[256,768]{1,0:T(8,128)(2,1)S(1)}, bf16[256,768]{1,0:T(8,128)(2,1)S(1)}, u32[]{:S(2)}, u32[]{:S(2)}) %collective-permute-start.31) | collective-permute-done | bytes 393248 | tf_op jit(solution)/shard_map/ppermute | solution.py:30
  92.7 2.7 %collective-permute-start.29 = (bf16[256,768]{1,0:T(8,128)(2,1)S(1)}, bf16[256,768]{1,0:T(8,128)(2,1)S(1)}, u32[]{:S(2)}, u32[]{:S(2)}) collective-permute-start(bf16[256,768]{1,0:T(8,128)(2,1)S(1)} %collective-permute-done.28.refs_3_), channel_id=1, source_target_pairs={{32,0},{64,32},{96,64},{128,96},{160,128},{192,160},{224,192},{0,2... | collective-permute-start | bytes 1179656 | tf_op jit(solution)/shard_map/ppermute | solution.py:30
  96.2 1.0 shard_map.97.refs_2_.glu_a.refs_0_
  97.6 1.0 shard_map.99
  98.6 3.7 %collective-permute-start.14 = (bf16[128,512]{1,0:T(8,128)(2,1)S(1)}, bf16[128,512]{1,0:T(8,128)(2,1)S(1)}, u32[]{:S(2)}, u32[]{:S(2)}) collective-permute-start(bf16[128,512]{1,0:T(8,128)(2,1)S(1)} %get-tuple-element.37), channel_id=1, source_target_pairs={{0,1},{1,0},{2,3},{3,2},{4,5},{5,4},{6,7},{7,6},{8,9},{9,8},{10,11... | collective-permute-start | bytes 393224 | tf_op jit(solution)/shard_map/ppermute | solution.py:34
  102.5 1.3 collective-permute-start.15
  103.8 1.2 shard_map.101
  105.9 8.0 %all_to_all.10 = f32[4,8,128]{2,1,0:T(8,128)S(1)} all-to-all(f32[4,8,128]{2,1,0:T(8,128)S(1)} %broadcast_in_dim.4), channel_id=1, replica_groups=mesh['z'=8,'y'=4,'x'=4,'c'=2] {'x'}, dimensions={0} | all-to-all | bytes 32768 | tf_op jit(solution)/shard_map/all_to_all | solution.py:302
  113.9 1.1 shard_map.103
  115.2 1.6 collective-permute-start.33
  120.1 17.5 %collective-permute-done.17.refs_2_ = bf16[96,2048]{1,0:T(8,128)(2,1)S(1)} collective-permute-done((bf16[96,2048]{1,0:T(8,128)(2,1)S(1)}, bf16[96,2048]{1,0:T(8,128)(2,1)S(1)}, u32[]{:S(2)}, u32[]{:S(2)}) %collective-permute-start.17) | collective-permute-done | bytes 393248 | tf_op jit(solution)/shard_map/ppermute | solution.py:30
  138.0 1.7 collective-permute-start.21
  139.7 1.2 collective-permute-start.22
  140.9 8.4 %collective-permute-done.20.m = bf16[96,2048]{1,0:T(8,128)(2,1)S(1)} collective-permute-done((bf16[96,2048]{1,0:T(8,128)(2,1)S(1)}, bf16[96,2048]{1,0:T(8,128)(2,1)S(1)}, u32[]{:S(2)}, u32[]{:S(2)}) %collective-permute-start.20) | collective-permute-done | bytes 393248 | tf_op jit(solution)/shard_map/ppermute | solution.py:30
  149.3 7.2 %collective-permute-done.21.f = bf16[96,2048]{1,0:T(8,128)(2,1)S(1)} collective-permute-done((bf16[96,2048]{1,0:T(8,128)(2,1)S(1)}, bf16[96,2048]{1,0:T(8,128)(2,1)S(1)}, u32[]{:S(2)}, u32[]{:S(2)}) %collective-permute-start.21) | collective-permute-done | bytes 393248 | tf_op jit(solution)/shard_map/ppermute | solution.py:30
  156.4 1.7 collective-permute-done.22.p
  158.5 1.0 shard_map.109.refs_2_.glu_a.refs_0_
  159.6 1.0 shard_map.110
  160.6 1.7 collective-permute-start.34
  162.3 3.9 %collective-permute-start.35 = (bf16[32,512]{1,0:T(8,128)(2,1)S(1)}, bf16[32,512]{1,0:T(8,128)(2,1)S(1)}, u32[]{:S(2)}, u32[]{:S(2)}) collective-permute-start(bf16[32,512]{1,0:T(8,128)(2,1)S(1)} %get-tuple-element.52), channel_id=1, source_target_pairs={{1,8},{9,16},{17,24},{25,32},{33,40},{41,48},{49,56},{57,64},{65,7... | collective-permute-start | bytes 98312 | tf_op jit(solution)/shard_map/ppermute | solution.py:287
  166.2 1.2 shard_map.111
  168.3 7.6 %all_to_all.11 = f32[4,8,128]{2,1,0:T(8,128)S(1)} all-to-all(f32[4,8,128]{2,1,0:T(8,128)S(1)} %broadcast_in_dim.5), channel_id=1, replica_groups=mesh['z'=8,'y'=4,'x'=4,'c'=2] {'x'}, dimensions={0} | all-to-all | bytes 32768 | tf_op jit(solution)/shard_map/all_to_all | solution.py:302
  175.9 1.1 shard_map.113
  177.3 2.4 %collective-permute-start.37 = (bf16[96,2048]{1,0:T(8,128)(2,1)S(1)}, bf16[96,2048]{1,0:T(8,128)(2,1)S(1)}, u32[]{:S(2)}, u32[]{:S(2)}) collective-permute-start(bf16[96,2048]{1,0:T(8,128)(2,1)S(1)} %get-tuple-element.60), channel_id=1, source_target_pairs={{2,0},{4,2},{6,4},{0,6},{3,1},{5,3},{7,5},{1,7},{10,8},{12,10},{14... | collective-permute-start | bytes 1179656 | tf_op jit(solution)/shard_map/ppermute | solution.py:30
  180.7 15.5 %collective-permute-done.36.refs_2_ = bf16[96,2048]{1,0:T(8,128)(2,1)S(1)} collective-permute-done((bf16[96,2048]{1,0:T(8,128)(2,1)S(1)}, bf16[96,2048]{1,0:T(8,128)(2,1)S(1)}, u32[]{:S(2)}, u32[]{:S(2)}) %collective-permute-start.36) | collective-permute-done | bytes 393248 | tf_op jit(solution)/shard_map/ppermute | solution.py:30
  (82 shorter events, 16.9 us)
Async XLA Ops:
  0.0 0.8 copy-start.1
  0.8 0.8 copy-start.2
  1.7 0.8 copy-start.3
  2.5 0.7 copy-start.5
  3.4 8.1 %collective-permute-start.3 = (bf16[64,768]{1,0:T(8,128)(2,1)S(1)}, bf16[64,768]{1,0:T(8,128)(2,1)S(1)}, u32[]{:S(2)}, u32[]{:S(2)}) collective-permute-start(bf16[64,768]{1,0:T(8,128)(2,1)S(1)} %get-tuple-element.35.own), channel_id=1, source_target_pairs={{32,0},{64,32},{96,64},{128,96},{160,128},{192,160},{224,192},{0,2... | collective-permute-start | bytes 294920 | tf_op jit(solution)/shard_map/ppermute | solution.py:30
  9.9 4.7 %collective-permute-start.4 = (bf16[64,768]{1,0:T(8,128)(2,1)S(1)}, bf16[64,768]{1,0:T(8,128)(2,1)S(1)}, u32[]{:S(2)}, u32[]{:S(2)}) collective-permute-start(bf16[64,768]{1,0:T(8,128)(2,1)S(1)} %get-tuple-element.35.own), channel_id=1, source_target_pairs={{224,0},{0,32},{32,64},{64,96},{96,128},{128,160},{160,192},{192,2... | collective-permute-start | bytes 294920 | tf_op jit(solution)/shard_map/ppermute | solution.py:30
  14.6 14.8 %collective-permute-start.5 = (bf16[128,768]{1,0:T(8,128)(2,1)S(1)}, bf16[128,768]{1,0:T(8,128)(2,1)S(1)}, u32[]{:S(2)}, u32[]{:S(2)}) collective-permute-start(bf16[128,768]{1,0:T(8,128)(2,1)S(1)} %get-tuple-element.62), channel_id=1, source_target_pairs={{64,0},{96,32},{128,64},{160,96},{192,128},{224,160},{0,192},{32,2... | collective-permute-start | bytes 589832 | tf_op jit(solution)/shard_map/ppermute | solution.py:30
  15.0 14.5 %collective-permute-start.7 = (bf16[128,768]{1,0:T(8,128)(2,1)S(1)}, bf16[128,768]{1,0:T(8,128)(2,1)S(1)}, u32[]{:S(2)}, u32[]{:S(2)}) collective-permute-start(bf16[128,768]{1,0:T(8,128)(2,1)S(1)} %get-tuple-element.61), channel_id=1, source_target_pairs={{192,0},{224,32},{0,64},{32,96},{64,128},{96,160},{128,192},{160,2... | collective-permute-start | bytes 589832 | tf_op jit(solution)/shard_map/ppermute | solution.py:30
  17.1 11.7 %collective-permute-start.6 = (bf16[64,768]{1,0:T(8,128)(2,1)S(1)}, bf16[64,768]{1,0:T(8,128)(2,1)S(1)}, u32[]{:S(2)}, u32[]{:S(2)}) collective-permute-start(bf16[64,768]{1,0:T(8,128)(2,1)S(1)} %get-tuple-element.35.own), channel_id=1, source_target_pairs={{128,0},{160,32},{192,64},{224,96},{0,128},{32,160},{64,192},{96,2... | collective-permute-start | bytes 294920 | tf_op jit(solution)/shard_map/ppermute | solution.py:30
  29.5 18.0 %collective-permute-start.8 = (bf16[512,768]{1,0:T(8,128)(2,1)S(1)}, bf16[512,768]{1,0:T(8,128)(2,1)S(1)}, u32[]{:S(2)}, u32[]{:S(2)}) collective-permute-start(bf16[512,768]{1,0:T(8,128)(2,1)S(1)} %shard_map.94.refs_0_), channel_id=1, source_target_pairs={{8,0},{16,8},{24,16},{0,24},{9,1},{17,9},{25,17},{1,25},{10,2},{18... | collective-permute-start | bytes 2359304 | tf_op jit(solution)/shard_map/ppermute | solution.py:30
  32.3 18.3 %collective-permute-start.10 = (bf16[512,768]{1,0:T(8,128)(2,1)S(1)}, bf16[512,768]{1,0:T(8,128)(2,1)S(1)}, u32[]{:S(2)}, u32[]{:S(2)}) collective-permute-start(bf16[512,768]{1,0:T(8,128)(2,1)S(1)} %shard_map.94.refs_0_), channel_id=1, source_target_pairs={{24,0},{0,8},{8,16},{16,24},{25,1},{1,9},{9,17},{17,25},{26,2},{2,... | collective-permute-start | bytes 2359304 | tf_op jit(solution)/shard_map/ppermute | solution.py:30
  50.8 13.1 %copy-start = (bf16[96,2048]{1,0:T(8,128)(2,1)S(1)}, bf16[96,2048]{1,0:T(8,128)(2,1)}, u32[]{:S(2)}) copy-start(bf16[96,2048]{1,0:T(8,128)(2,1)} %refs_0_.2) | copy-start | bytes 1179652
  50.8 46.4 %collective-permute-start.12 = (bf16[1536,768]{1,0:T(8,128)(2,1)S(1)}, bf16[1536,768]{1,0:T(8,128)(2,1)S(1)}, u32[]{:S(2)}, u32[]{:S(2)}) collective-permute-start(bf16[1536,768]{1,0:T(8,128)(2,1)S(1)} %pad_maximum_fusion), channel_id=1, source_target_pairs={{0,1},{1,0},{2,3},{3,2},{4,5},{5,4},{6,7},{7,6},{8,9},{9,8},{10,11... | collective-permute-start | bytes 7077896 | tf_op jit(solution)/shard_map/ppermute | solution.py:34
  53.8 4.3 %collective-permute-start.23 = (bf16[64,768]{1,0:T(8,128)(2,1)S(1)}, bf16[64,768]{1,0:T(8,128)(2,1)S(1)}, u32[]{:S(2)}, u32[]{:S(2)}) collective-permute-start(bf16[64,768]{1,0:T(8,128)(2,1)S(1)} %get-tuple-element.49.refs_0_), channel_id=1, source_target_pairs={{8,0},{16,8},{24,16},{0,24},{9,1},{17,9},{25,17},{1,25},{10,2},{18... | collective-permute-start | bytes 294920 | tf_op jit(solution)/shard_map/ppermute | solution.py:30
  53.8 5.5 %collective-permute-start.24 = (bf16[64,768]{1,0:T(8,128)(2,1)S(1)}, bf16[64,768]{1,0:T(8,128)(2,1)S(1)}, u32[]{:S(2)}, u32[]{:S(2)}) collective-permute-start(bf16[64,768]{1,0:T(8,128)(2,1)S(1)} %get-tuple-element.49.refs_0_), channel_id=1, source_target_pairs={{16,0},{24,8},{0,16},{8,24},{17,1},{25,9},{1,17},{9,25},{18,2},{26... | collective-permute-start | bytes 294920 | tf_op jit(solution)/shard_map/ppermute | solution.py:30
  54.3 7.8 %collective-permute-start.25 = (bf16[64,768]{1,0:T(8,128)(2,1)S(1)}, bf16[64,768]{1,0:T(8,128)(2,1)S(1)}, u32[]{:S(2)}, u32[]{:S(2)}) collective-permute-start(bf16[64,768]{1,0:T(8,128)(2,1)S(1)} %get-tuple-element.49.refs_0_), channel_id=1, source_target_pairs={{24,0},{0,8},{8,16},{16,24},{25,1},{1,9},{9,17},{17,25},{26,2},{2,... | collective-permute-start | bytes 294920 | tf_op jit(solution)/shard_map/ppermute | solution.py:30
  62.2 10.3 %collective-permute-start.26 = (bf16[256,768]{1,0:T(8,128)(2,1)S(1)}, bf16[256,768]{1,0:T(8,128)(2,1)S(1)}, u32[]{:S(2)}, u32[]{:S(2)}) collective-permute-start(bf16[256,768]{1,0:T(8,128)(2,1)S(1)} %shard_map.107.refs_0_), channel_id=1, source_target_pairs={{32,0},{64,32},{96,64},{128,96},{160,128},{192,160},{224,192},{0,2... | collective-permute-start | bytes 1179656 | tf_op jit(solution)/shard_map/ppermute | solution.py:30
  62.3 11.4 %collective-permute-start.9 = (bf16[256,768]{1,0:T(8,128)(2,1)S(1)}, bf16[256,768]{1,0:T(8,128)(2,1)S(1)}, u32[]{:S(2)}, u32[]{:S(2)}) collective-permute-start(bf16[256,768]{1,0:T(8,128)(2,1)S(1)} %slice.8), channel_id=1, source_target_pairs={{8,0},{16,8},{24,16},{0,24},{9,1},{17,9},{25,17},{1,25},{10,2},{18... | collective-permute-start | bytes 1179656 | tf_op jit(solution)/shard_map/ppermute | solution.py:30
  62.8 12.5 %collective-permute-start.11 = (bf16[256,768]{1,0:T(8,128)(2,1)S(1)}, bf16[256,768]{1,0:T(8,128)(2,1)S(1)}, u32[]{:S(2)}, u32[]{:S(2)}) collective-permute-start(bf16[256,768]{1,0:T(8,128)(2,1)S(1)} %slice.9), channel_id=1, source_target_pairs={{24,0},{0,8},{8,16},{16,24},{25,1},{1,9},{9,17},{17,25},{26,2},{2,... | collective-permute-start | bytes 1179656 | tf_op jit(solution)/shard_map/ppermute | solution.py:30
  64.0 14.1 %collective-permute-start = (bf16[96,2048]{1,0:T(8,128)(2,1)S(1)}, bf16[96,2048]{1,0:T(8,128)(2,1)S(1)}, u32[]{:S(2)}, u32[]{:S(2)}) collective-permute-start(bf16[96,2048]{1,0:T(8,128)(2,1)S(1)} %shard_map.91.own.refs_0_), channel_id=1, source_target_pairs={{6,0},{0,2},{2,4},{4,6},{7,1},{1,3},{3,5},{5,7},{14,8},{8,10},{10,... | collective-permute-start | bytes 1179656 | tf_op jit(solution)/shard_map/ppermute | solution.py:30
  72.4 10.6 %collective-permute-start.30 = (bf16[256,768]{1,0:T(8,128)(2,1)S(1)}, bf16[256,768]{1,0:T(8,128)(2,1)S(1)}, u32[]{:S(2)}, u32[]{:S(2)}) collective-permute-start(bf16[256,768]{1,0:T(8,128)(2,1)S(1)} %shard_map.107.refs_0_), channel_id=1, source_target_pairs={{224,0},{0,32},{32,64},{64,96},{96,128},{128,160},{160,192},{192,2... | collective-permute-start | bytes 1179656 | tf_op jit(solution)/shard_map/ppermute | solution.py:30
  73.7 9.6 %collective-permute-start.27 = (bf16[256,768]{1,0:T(8,128)(2,1)S(1)}, bf16[256,768]{1,0:T(8,128)(2,1)S(1)}, u32[]{:S(2)}, u32[]{:S(2)}) collective-permute-start(bf16[256,768]{1,0:T(8,128)(2,1)S(1)} %collective-permute-done.26.refs_1_), channel_id=1, source_target_pairs={{32,0},{64,32},{96,64},{128,96},{160,128},{192,160},{224,192},{0,2... | collective-permute-start | bytes 1179656 | tf_op jit(solution)/shard_map/ppermute | solution.py:30
  75.3 10.4 %collective-permute-start.1 = (bf16[96,2048]{1,0:T(8,128)(2,1)S(1)}, bf16[96,2048]{1,0:T(8,128)(2,1)S(1)}, u32[]{:S(2)}, u32[]{:S(2)}) collective-permute-start(bf16[96,2048]{1,0:T(8,128)(2,1)S(1)} %shard_map.91.own.refs_0_), channel_id=1, source_target_pairs={{4,0},{6,2},{0,4},{2,6},{5,1},{7,3},{1,5},{3,7},{12,8},{14,10},{8,... | collective-permute-start | bytes 1179656 | tf_op jit(solution)/shard_map/ppermute | solution.py:30
  78.1 19.1 %collective-permute-start.13 = (bf16[512,768]{1,0:T(8,128)(2,1)S(1)}, bf16[512,768]{1,0:T(8,128)(2,1)S(1)}, u32[]{:S(2)}, u32[]{:S(2)}) collective-permute-start(bf16[512,768]{1,0:T(8,128)(2,1)S(1)} %pad_maximum_fusion.1), channel_id=1, source_target_pairs={{0,1},{1,0},{2,3},{3,2},{4,5},{5,4},{6,7},{7,6},{8,9},{9,8},{10,11... | collective-permute-start | bytes 2359304 | tf_op jit(solution)/shard_map/ppermute | solution.py:34
  83.0 9.7 %collective-permute-start.31 = (bf16[256,768]{1,0:T(8,128)(2,1)S(1)}, bf16[256,768]{1,0:T(8,128)(2,1)S(1)}, u32[]{:S(2)}, u32[]{:S(2)}) collective-permute-start(bf16[256,768]{1,0:T(8,128)(2,1)S(1)} %collective-permute-done.30.refs_7_), channel_id=1, source_target_pairs={{224,0},{0,32},{32,64},{64,96},{96,128},{128,160},{160,192},{192,2... | collective-permute-start | bytes 1179656 | tf_op jit(solution)/shard_map/ppermute | solution.py:30
  83.3 9.4 %collective-permute-start.28 = (bf16[256,768]{1,0:T(8,128)(2,1)S(1)}, bf16[256,768]{1,0:T(8,128)(2,1)S(1)}, u32[]{:S(2)}, u32[]{:S(2)}) collective-permute-start(bf16[256,768]{1,0:T(8,128)(2,1)S(1)} %collective-permute-done.27.refs_2_), channel_id=1, source_target_pairs={{32,0},{64,32},{96,64},{128,96},{160,128},{192,160},{224,192},{0,2... | collective-permute-start | bytes 1179656 | tf_op jit(solution)/shard_map/ppermute | solution.py:30
  85.7 9.7 %collective-permute-start.2 = (bf16[96,2048]{1,0:T(8,128)(2,1)S(1)}, bf16[96,2048]{1,0:T(8,128)(2,1)S(1)}, u32[]{:S(2)}, u32[]{:S(2)}) collective-permute-start(bf16[96,2048]{1,0:T(8,128)(2,1)S(1)} %shard_map.91.own.refs_0_), channel_id=1, source_target_pairs={{2,0},{4,2},{6,4},{0,6},{3,1},{5,3},{7,5},{1,7},{10,8},{12,10},{14... | collective-permute-start | bytes 1179656 | tf_op jit(solution)/shard_map/ppermute | solution.py:30
  92.7 22.3 %collective-permute-start.32 = (bf16[256,768]{1,0:T(8,128)(2,1)S(1)}, bf16[256,768]{1,0:T(8,128)(2,1)S(1)}, u32[]{:S(2)}, u32[]{:S(2)}) collective-permute-start(bf16[256,768]{1,0:T(8,128)(2,1)S(1)} %collective-permute-done.31.refs_6_), channel_id=1, source_target_pairs={{224,0},{0,32},{32,64},{64,96},{96,128},{128,160},{160,192},{192,2... | collective-permute-start | bytes 1179656 | tf_op jit(solution)/shard_map/ppermute | solution.py:30
  92.7 22.3 %collective-permute-start.29 = (bf16[256,768]{1,0:T(8,128)(2,1)S(1)}, bf16[256,768]{1,0:T(8,128)(2,1)S(1)}, u32[]{:S(2)}, u32[]{:S(2)}) collective-permute-start(bf16[256,768]{1,0:T(8,128)(2,1)S(1)} %collective-permute-done.28.refs_3_), channel_id=1, source_target_pairs={{32,0},{64,32},{96,64},{128,96},{160,128},{192,160},{224,192},{0,2... | collective-permute-start | bytes 1179656 | tf_op jit(solution)/shard_map/ppermute | solution.py:30
  97.5 4.8 %copy-start.4 = (f32[2,31,256]{2,0,1:T(2,128)S(1)}, f32[2,31,256]{2,0,1:T(2,128)}, u32[]{:S(2)}) copy-start(f32[2,31,256]{2,0,1:T(2,128)} %param.13) | copy-start | bytes 190468
  97.6 4.8 %copy-start.6 = (f32[2,256]{1,0:T(2,128)S(1)}, f32[2,256]{1,0:T(2,128)}, u32[]{:S(2)}) copy-start(f32[2,256]{1,0:T(2,128)} %cb.1) | copy-start | bytes 6148
  97.6 4.7 %copy-start.7 = (f32[2,256]{1,0:T(2,128)S(1)}, f32[2,256]{1,0:T(2,128)}, u32[]{:S(2)}) copy-start(f32[2,256]{1,0:T(2,128)} %cg.1) | copy-start | bytes 6148
  97.6 4.7 %copy-start.8 = (f32[2,256]{1,0:T(2,128)S(1)}, f32[2,256]{1,0:T(2,128)}, u32[]{:S(2)}) copy-start(f32[2,256]{1,0:T(2,128)} %cs.1) | copy-start | bytes 6148
  98.6 6.4 %collective-permute-start.14 = (bf16[128,512]{1,0:T(8,128)(2,1)S(1)}, bf16[128,512]{1,0:T(8,128)(2,1)S(1)}, u32[]{:S(2)}, u32[]{:S(2)}) collective-permute-start(bf16[128,512]{1,0:T(8,128)(2,1)S(1)} %get-tuple-element.37), channel_id=1, source_target_pairs={{0,1},{1,0},{2,3},{3,2},{4,5},{5,4},{6,7},{7,6},{8,9},{9,8},{10,11... | collective-permute-start | bytes 393224 | tf_op jit(solution)/shard_map/ppermute | solution.py:34
  102.4 1.4 collective-permute-start.16
  102.5 2.5 %collective-permute-start.15 = (bf16[32,512]{1,0:T(8,128)(2,1)S(1)}, bf16[32,512]{1,0:T(8,128)(2,1)S(1)}, u32[]{:S(2)}, u32[]{:S(2)}) collective-permute-start(bf16[32,512]{1,0:T(8,128)(2,1)S(1)} %get-tuple-element.38), channel_id=1, source_target_pairs={{1,8},{9,16},{17,24},{25,32},{33,40},{41,48},{49,56},{57,64},{65,7... | collective-permute-start | bytes 98312 | tf_op jit(solution)/shard_map/ppermute | solution.py:287
  115.2 44.4 %collective-permute-start.33 = (bf16[2048,768]{1,0:T(8,128)(2,1)S(1)}, bf16[2048,768]{1,0:T(8,128)(2,1)S(1)}, u32[]{:S(2)}, u32[]{:S(2)}) collective-permute-start(bf16[2048,768]{1,0:T(8,128)(2,1)S(1)} %shard_map.108.w.refs_5_), channel_id=1, source_target_pairs={{0,1},{1,0},{2,3},{3,2},{4,5},{5,4},{6,7},{7,6},{8,9},{9,8},{10,11... | collective-permute-start | bytes 9437192 | tf_op jit(solution)/shard_map/ppermute | solution.py:34
  116.8 20.8 %collective-permute-start.18 = (bf16[96,2048]{1,0:T(8,128)(2,1)S(1)}, bf16[96,2048]{1,0:T(8,128)(2,1)S(1)}, u32[]{:S(2)}, u32[]{:S(2)}) collective-permute-start(bf16[96,2048]{1,0:T(8,128)(2,1)S(1)} %get-tuple-element.46.refs_8_), channel_id=1, source_target_pairs={{2,0},{4,2},{6,4},{0,6},{3,1},{5,3},{7,5},{1,7},{10,8},{12,10},{14... | collective-permute-start | bytes 1179656 | tf_op jit(solution)/shard_map/ppermute | solution.py:30
  117.7 19.9 %collective-permute-start.17 = (bf16[96,2048]{1,0:T(8,128)(2,1)S(1)}, bf16[96,2048]{1,0:T(8,128)(2,1)S(1)}, u32[]{:S(2)}, u32[]{:S(2)}) collective-permute-start(bf16[96,2048]{1,0:T(8,128)(2,1)S(1)} %get-tuple-element.45), channel_id=1, source_target_pairs={{6,0},{0,2},{2,4},{4,6},{7,1},{1,3},{3,5},{5,7},{14,8},{8,10},{10,... | collective-permute-start | bytes 1179656 | tf_op jit(solution)/shard_map/ppermute | solution.py:30
  119.2 18.5 %collective-permute-start.19 = (bf16[96,2048]{1,0:T(8,128)(2,1)S(1)}, bf16[96,2048]{1,0:T(8,128)(2,1)S(1)}, u32[]{:S(2)}, u32[]{:S(2)}) collective-permute-start(bf16[96,2048]{1,0:T(8,128)(2,1)S(1)} %shard_map.104), channel_id=1, source_target_pairs={{4,0},{6,2},{0,4},{2,6},{5,1},{7,3},{1,5},{3,7},{12,8},{14,10},{8,... | collective-permute-start | bytes 1179656 | tf_op jit(solution)/shard_map/ppermute | solution.py:30
  137.9 11.4 %collective-permute-start.20 = (bf16[96,2048]{1,0:T(8,128)(2,1)S(1)}, bf16[96,2048]{1,0:T(8,128)(2,1)S(1)}, u32[]{:S(2)}, u32[]{:S(2)}) collective-permute-start(bf16[96,2048]{1,0:T(8,128)(2,1)S(1)} %shard_map.105.own.refs_0_), channel_id=1, source_target_pairs={{6,0},{0,2},{2,4},{4,6},{7,1},{1,3},{3,5},{5,7},{14,8},{8,10},{10,... | collective-permute-start | bytes 1179656 | tf_op jit(solution)/shard_map/ppermute | solution.py:30
  138.0 18.5 %collective-permute-start.21 = (bf16[96,2048]{1,0:T(8,128)(2,1)S(1)}, bf16[96,2048]{1,0:T(8,128)(2,1)S(1)}, u32[]{:S(2)}, u32[]{:S(2)}) collective-permute-start(bf16[96,2048]{1,0:T(8,128)(2,1)S(1)} %shard_map.105.own.refs_0_), channel_id=1, source_target_pairs={{4,0},{6,2},{0,4},{2,6},{5,1},{7,3},{1,5},{3,7},{12,8},{14,10},{8,... | collective-permute-start | bytes 1179656 | tf_op jit(solution)/shard_map/ppermute | solution.py:30
  139.7 18.4 %collective-permute-start.22 = (bf16[96,2048]{1,0:T(8,128)(2,1)S(1)}, bf16[96,2048]{1,0:T(8,128)(2,1)S(1)}, u32[]{:S(2)}, u32[]{:S(2)}) collective-permute-start(bf16[96,2048]{1,0:T(8,128)(2,1)S(1)} %shard_map.105.own.refs_0_), channel_id=1, source_target_pairs={{2,0},{4,2},{6,4},{0,6},{3,1},{5,3},{7,5},{1,7},{10,8},{12,10},{14... | collective-permute-start | bytes 1179656 | tf_op jit(solution)/shard_map/ppermute | solution.py:30
  160.6 6.8 %collective-permute-start.34 = (bf16[128,512]{1,0:T(8,128)(2,1)S(1)}, bf16[128,512]{1,0:T(8,128)(2,1)S(1)}, u32[]{:S(2)}, u32[]{:S(2)}) collective-permute-start(bf16[128,512]{1,0:T(8,128)(2,1)S(1)} %get-tuple-element.51), channel_id=1, source_target_pairs={{0,1},{1,0},{2,3},{3,2},{4,5},{5,4},{6,7},{7,6},{8,9},{9,8},{10,11... | collective-permute-start | bytes 393224 | tf_op jit(solution)/shard_map/ppermute | solution.py:34
  162.3 5.1 %collective-permute-start.35 = (bf16[32,512]{1,0:T(8,128)(2,1)S(1)}, bf16[32,512]{1,0:T(8,128)(2,1)S(1)}, u32[]{:S(2)}, u32[]{:S(2)}) collective-permute-start(bf16[32,512]{1,0:T(8,128)(2,1)S(1)} %get-tuple-element.52), channel_id=1, source_target_pairs={{1,8},{9,16},{17,24},{25,32},{33,40},{41,48},{49,56},{57,64},{65,7... | collective-permute-start | bytes 98312 | tf_op jit(solution)/shard_map/ppermute | solution.py:287
  177.0 19.2 %collective-permute-start.36 = (bf16[96,2048]{1,0:T(8,128)(2,1)S(1)}, bf16[96,2048]{1,0:T(8,128)(2,1)S(1)}, u32[]{:S(2)}, u32[]{:S(2)}) collective-permute-start(bf16[96,2048]{1,0:T(8,128)(2,1)S(1)} %get-tuple-element.59), channel_id=1, source_target_pairs={{6,0},{0,2},{2,4},{4,6},{7,1},{1,3},{3,5},{5,7},{14,8},{8,10},{10,... | collective-permute-start | bytes 1179656 | tf_op jit(solution)/shard_map/ppermute | solution.py:30
  177.3 18.9 %collective-permute-start.37 = (bf16[96,2048]{1,0:T(8,128)(2,1)S(1)}, bf16[96,2048]{1,0:T(8,128)(2,1)S(1)}, u32[]{:S(2)}, u32[]{:S(2)}) collective-permute-start(bf16[96,2048]{1,0:T(8,128)(2,1)S(1)} %get-tuple-element.60), channel_id=1, source_target_pairs={{2,0},{4,2},{6,4},{0,6},{3,1},{5,3},{7,5},{1,7},{10,8},{12,10},{14... | collective-permute-start | bytes 1179656 | tf_op jit(solution)/shard_map/ppermute | solution.py:30
  180.6 15.6 %collective-permute-start.38 = (bf16[96,2048]{1,0:T(8,128)(2,1)S(1)}, bf16[96,2048]{1,0:T(8,128)(2,1)S(1)}, u32[]{:S(2)}, u32[]{:S(2)}) collective-permute-start(bf16[96,2048]{1,0:T(8,128)(2,1)S(1)} %shard_map.114), channel_id=1, source_target_pairs={{4,0},{6,2},{0,4},{2,6},{5,1},{7,3},{1,5},{3,7},{12,8},{14,10},{8,... | collective-permute-start | bytes 1179656 | tf_op jit(solution)/shard_map/ppermute | solution.py:30
